TPU v7x, 32 devices: a whole 2x2x4 slice. The times are simulated.
32 devices in a mesh: sp: 16 (over z, y, x), tp: 2 (over core).
Axes of the slice: x: 2, y: 2, z: 4, core: 2. Of those that a mesh axis runs over, the one named last changes fastest.
Arguments:
- tokens: bfloat16 [4096, 4096], P('sp'), may hold values from -5 to 5
- documents: int32 [4096], P('sp'), may hold values from 0 to 3, never falling along the last dimension, each value on 1 to 2048 neighbouring positions
- norm_gain: float32 [2, 4096], replicated, may hold values from 0.1 to 1.9
- in_weight: bfloat16 [2, 4096, 2048], P(None, 'sp', 'tp'), may hold values from -0.09375 to 0.09375
- conv_taps: float32 [2, 4, 2048], P(None, None, 'tp'), may hold values from -3 to 3
- conv_bias: float32 [2, 2048], P(None, 'tp'), may hold values from -0.75 to 0.75
- recur_gate: bfloat16 [2, 32, 64, 64], P(None, 'tp'), may hold values from -0.75 to 0.75
- input_gate: bfloat16 [2, 32, 64, 64], P(None, 'tp'), may hold values from -0.75 to 0.75
- recur_bias: float32 [2, 2048], P(None, 'tp'), may hold values from -4 to 4
- input_bias: float32 [2, 2048], P(None, 'tp'), may hold values from -4 to 4
- decay_param: float32 [2, 2048], P(None, 'tp'), may hold values from 4 to 7
- out_weight: bfloat16 [2, 2048, 4096], P(None, 'tp', 'sp'), may hold values from -0.375 to 0.375
Outputs:
- layered: bfloat16 [4096, 4096], P('sp')
All inputs are finite; a program needn't handle non-finite values.
Results may differ from a plain program's by a relative error of at most 0.017.
Values may be sent and summed in bfloat16 or wider, within the bound.
A program may use at most 128 MiB of HBM per device.

v0:
```python
import jax
import jax.numpy as jnp
from jax import lax
from jax.sharding import PartitionSpec as P

RG_C = 8.0
EPS = 0.1


def passed_along(block, axis, distance):
    devices = range(lax.axis_size(axis))
    route = [(i - distance, i) for i in devices if i - distance in devices]
    return lax.ppermute(block, axis, route)


def carried_in(part, axis, combine, identity):
    place = lax.axis_index(axis)
    gathered = jax.tree.map(lambda a: lax.all_gather(a, axis), part)
    state = jax.tree.map(lambda a, e: jnp.zeros_like(a) + jnp.asarray(e, a.dtype), part, identity)

    def one(hop, state):
        return combine(
            state, jax.tree.map(lambda a: lax.dynamic_index_in_dim(a, hop, 0, False), gathered)
        )

    return lax.fori_loop(0, place, one, state)


def norm_rows(values_in, gain_row):
    values = values_in.astype(jnp.float32)
    scaled = values * lax.rsqrt(jnp.mean(values * values, axis=-1, keepdims=True) + EPS)
    return (scaled * gain_row[None, :]).astype(jnp.bfloat16)


def combine(earlier, following):
    return (earlier[0] * following[0], following[0] * earlier[1] + following[1])


def per_device(
    tokens,
    documents,
    norm_gain,
    in_weight,
    conv_taps,
    conv_bias,
    recur_gate,
    input_gate,
    recur_bias,
    input_bias,
    decay_param,
    out_weight,
):
    num_rows = tokens.shape[0]
    layer_count = in_weight.shape[0]
    chan_width = in_weight.shape[2]
    tap_count = conv_taps.shape[1]
    blocks = recur_gate.shape[1]
    block_dim = recur_gate.shape[2]
    doc_values = documents.astype(jnp.bfloat16)
    whole_in, whole_out = (
        lax.all_gather(in_weight, "sp", axis=1, tiled=True),
        lax.all_gather(out_weight, "sp", axis=2, tiled=True),
    )
    state_x = tokens
    for depth_at in range(layer_count):
        normed = norm_rows(state_x, norm_gain[depth_at])
        projected = jnp.dot(normed, whole_in[depth_at], preferred_element_type=jnp.float32)
        mixed_in = projected.astype(jnp.bfloat16)
        cut_at = num_rows - tap_count + 1
        tail_in, tail_doc = passed_along((mixed_in[cut_at:], doc_values[cut_at:]), "sp", 1)
        ext_in = jnp.concatenate([tail_in, mixed_in], axis=0).astype(jnp.float32)
        ext_doc = jnp.concatenate([tail_doc, doc_values], axis=0)
        first = tap_count - 1
        conv_sum = conv_bias[depth_at][None, :] + conv_taps[depth_at, 0][None, :] * ext_in[first:]
        for lag_step in range(1, tap_count):
            low = first - lag_step
            same_doc = (ext_doc[low : low + num_rows] == doc_values)[:, None]
            conv_sum = conv_sum + jnp.where(
                same_doc, conv_taps[depth_at, lag_step][None, :] * ext_in[low : low + num_rows], 0.0
            )
        conv_out = conv_sum.astype(jnp.bfloat16)
        grouped = conv_out.reshape(num_rows, blocks, block_dim)
        recur_rate = jax.nn.sigmoid(
            jnp.einsum(
                "snb,nbc->snc", grouped, recur_gate[depth_at], preferred_element_type=jnp.float32
            ).reshape(num_rows, chan_width)
            + recur_bias[depth_at][None, :]
        )
        input_rate = jax.nn.sigmoid(
            jnp.einsum(
                "snb,nbc->snc", grouped, input_gate[depth_at], preferred_element_type=jnp.float32
            ).reshape(num_rows, chan_width)
            + input_bias[depth_at][None, :]
        )
        reset = ext_doc[first - 1 : first - 1 + num_rows] != doc_values
        log_decay = -RG_C * jax.nn.softplus(-decay_param[depth_at])[None, :] * recur_rate
        decay_now = jnp.where(reset[:, None], 0.0, jnp.exp(log_decay))
        drive_term = jnp.sqrt(jnp.maximum(-jnp.expm1(2.0 * log_decay), 0.0)) * (
            input_rate * conv_out.astype(jnp.float32)
        )
        cum_decay, local_state = lax.associative_scan(combine, (decay_now, drive_term), axis=0)
        identity = (jnp.ones((chan_width,), jnp.float32), jnp.zeros((chan_width,), jnp.float32))
        _, carried = carried_in(
            (cum_decay[num_rows - 1], local_state[num_rows - 1]), "sp", combine, identity
        )
        hidden = (local_state + cum_decay * carried[None, :]).astype(jnp.bfloat16)
        partial_sum = jnp.dot(hidden, whole_out[depth_at], preferred_element_type=jnp.float32)
        summed = lax.psum(partial_sum.astype(jnp.bfloat16), "tp").astype(jnp.float32)
        state_x = (state_x.astype(jnp.float32) + summed).astype(jnp.bfloat16)
    return state_x


def solution(mesh):
    return jax.shard_map(
        per_device,
        mesh=mesh,
        in_specs=(
            P("sp", None),
            P("sp"),
            P(),
            P(None, "sp", "tp"),
            P(None, None, "tp"),
            P(None, "tp"),
            P(None, "tp", None, None),
            P(None, "tp", None, None),
            P(None, "tp"),
            P(None, "tp"),
            P(None, "tp"),
            P(None, "tp", "sp"),
        ),
        out_specs=P("sp", None),
        check_vma=False,
    )
```

profile of v0, /device:TPU:0, one launch (start us, length us, event | category | flops | bytes accessed | tf_op | source)
XLA Modules:
  0.0 754.7 jit_solution(14435381683469304299)
XLA Ops:
  8.9 4.9 collective-permute-start.1
  13.7 2.1 fusion.6
  19.6 184.4 %all-gather.7.cloned.1.call-done = bf16[2,4096,1024]{2,1,0:T(8,128)(2,1)} async-done(((bf16[2,256,1024]{2,1,0:T(8,128)(2,1)}), bf16[2,4096,1024]{2,1,0:T(8,128)(2,1)}) %all-gather.7.cloned.1.call-update) | async-done | bytes 16777232 | tf_op jit(solution)/shard_map/all_gather | solution.py:61
  204.0 5.8 fusion.20
  209.8 3.0 collective-permute-start
  215.7 2.1 copy.35
  217.8 2.4 fusion.54
  220.2 2.5 copy.37
  222.7 2.4 fusion.52
  225.2 2.5 copy.39
  227.7 4.2 multiply_multiply_fusion.1
  232.0 2.1 slice.622
  234.0 3.3 slice.623
  237.3 3.2 slice.621
  240.5 3.3 slice.625
  243.8 2.3 multiply_add_fusion.3
  247.8 1.8 slice.627
  251.4 2.0 multiply_add_fusion.5
  258.0 1.8 multiply_add_fusion.7
  302.4 1.8 slice.626
  310.2 3.3 slice.677
  326.6 1.8 fusion.47
  330.4 4.7 pad.211
  336.8 2.6 pad.224
  341.0 2.1 add.517
  343.1 2.6 fusion.43
  345.8 2.8 pad.210
  349.3 41.5 %all-gather.1 = f32[16,1,1024]{2,1,0:T(1,128)S(1)} all-gather(f32[1,1,1024]{2,1,0:T(1,128)S(1)} %add_bitcast_fusion.2), channel_id=1, replica_groups=mesh['sp'=16,'tp'=2] {'sp'}, dimensions={0}, use_global_device_ids=true | all-gather | bytes 69632 | tf_op jit(solution)/shard_map/all_gather | solution.py:18
  390.9 4.6 pad.227
  395.6 2.7 pad.226
  399.1 46.4 %all-gather = f32[16,1,1024]{2,1,0:T(1,128)S(1)} all-gather(f32[1,1,1024]{2,1,0:T(1,128)S(1)} %add_bitcast_fusion.3), channel_id=1, replica_groups=mesh['sp'=16,'tp'=2] {'sp'}, dimensions={0}, use_global_device_ids=true | all-gather | bytes 69632 | tf_op jit(solution)/shard_map/all_gather | solution.py:18
  445.8 8.5 %fusion.4 = bf16[256,4096]{1,0:T(8,128)(2,1)} fusion(bf16[2,1024,4096]{2,1,0:T(8,128)(2,1)} %all-gather.9.cloned.1.call-done, f32[256,1024]{1,0:T(8,128)} %pad.226, f32[256,1024]{1,0:T(8,128)} %pad.227, f32[256,1024]{1,0:T(8,128)} %pad.210, f32[256,1024]{1,0:T(8,128)} %pad.211, f32[1024]{0:T(1024)S(1)} %get-tuple-element.93), kind=kOutput, calls=%fused_computation.20 | convolution fusion | flops 2149842944 | bytes 14684160 | tf_op jit(solution)/shard_map/dot_general | solution.py:107
  454.4 20.7 %all-reduce.67.cloned.1.call-done = bf16[256,4096]{1,0:T(8,128)(2,1)} async-done(((bf16[256,4096]{1,0:T(8,128)(2,1)}), bf16[256,4096]{1,0:T(8,128)(2,1)}) %all-reduce.67.cloned.1.call-update) | async-done | bytes 2097168 | tf_op jit(solution)/shard_map/psum | solution.py:108
  475.1 2.5 fusion.10
  477.7 5.8 fusion.23
  484.4 3.6 collective-permute-start.2
  492.1 2.1 copy.40
  494.1 2.5 fusion.50
  496.6 2.4 fusion.48
  499.1 2.5 copy.42
  501.6 2.6 copy.44
  504.2 4.2 multiply_multiply_fusion
  508.4 2.1 slice.716
  510.5 3.3 slice.717
  513.7 3.3 slice.715
  517.0 3.2 slice.719
  520.2 2.3 multiply_add_fusion.2
  524.2 1.8 slice.721
  527.6 2.0 multiply_add_fusion.4
  534.2 1.8 multiply_add_fusion.6
  589.1 3.3 slice.771
  606.6 1.8 fusion.46
  610.4 4.6 pad.243
  616.7 2.6 pad.256
  620.9 2.1 add.566
  623.0 2.6 fusion.42
  625.7 2.7 pad.242
  629.1 41.7 %all-gather.3 = f32[16,1,1024]{2,1,0:T(1,128)S(1)} all-gather(f32[1,1,1024]{2,1,0:T(1,128)S(1)} %add_bitcast_fusion), channel_id=1, replica_groups=mesh['sp'=16,'tp'=2] {'sp'}, dimensions={0}, use_global_device_ids=true | all-gather | bytes 69632 | tf_op jit(solution)/shard_map/all_gather | solution.py:18
  670.9 4.6 pad.259
  675.6 2.7 pad.258
  679.1 35.8 %all-gather.2 = f32[16,1,1024]{2,1,0:T(1,128)S(1)} all-gather(f32[1,1,1024]{2,1,0:T(1,128)S(1)} %add_bitcast_fusion.1), channel_id=1, replica_groups=mesh['sp'=16,'tp'=2] {'sp'}, dimensions={0}, use_global_device_ids=true | all-gather | bytes 69632 | tf_op jit(solution)/shard_map/all_gather | solution.py:18
  715.0 8.4 %fusion.5 = bf16[256,4096]{1,0:T(8,128)(2,1)} fusion(bf16[2,1024,4096]{2,1,0:T(8,128)(2,1)} %all-gather.9.cloned.1.call-done, f32[256,1024]{1,0:T(8,128)} %pad.258, f32[256,1024]{1,0:T(8,128)} %pad.259, f32[256,1024]{1,0:T(8,128)} %pad.242, f32[256,1024]{1,0:T(8,128)} %pad.243, f32[1024]{0:T(1024)S(1)} %get-tuple-element.94), kind=kOutput, calls=%fused_computation.21 | convolution fusion | flops 2149842944 | bytes 14684160 | tf_op jit(solution)/shard_map/dot_general | solution.py:107
  723.4 20.1 %all-reduce.69.cloned.1.call-done = bf16[256,4096]{1,0:T(8,128)(2,1)} async-done(((bf16[256,4096]{1,0:T(8,128)(2,1)}), bf16[256,4096]{1,0:T(8,128)(2,1)}) %all-reduce.69.cloned.1.call-update) | async-done | bytes 2097168 | tf_op jit(solution)/shard_map/psum | solution.py:108
  743.5 4.7 fusion.13
  (337 shorter events, 172.6 us)
Async XLA Ops:
  6.5 197.4 %copy-start = (bf16[256,4096]{1,0:T(8,128)(2,1)S(1)}, bf16[256,4096]{1,0:T(8,128)(2,1)}, u32[]{:S(2)}) copy-start(bf16[256,4096]{1,0:T(8,128)(2,1)} %param.16) | copy-start | bytes 6291460
  6.5 9.3 %copy-start.36 = (f32[2,1024]{1,0:T(2,128)S(1)}, f32[2,1024]{1,0:T(2,128)}, u32[]{:S(2)}) copy-start(f32[2,1024]{1,0:T(2,128)} %param.21) | copy-start | bytes 24580
  6.5 9.9 %copy-start.37 = (f32[2,1024]{1,0:T(2,128)S(1)}, f32[2,1024]{1,0:T(2,128)}, u32[]{:S(2)}) copy-start(f32[2,1024]{1,0:T(2,128)} %param.24) | copy-start | bytes 24580
  6.5 10.5 %copy-start.38 = (f32[2,1024]{1,0:T(2,128)S(1)}, f32[2,1024]{1,0:T(2,128)}, u32[]{:S(2)}) copy-start(f32[2,1024]{1,0:T(2,128)} %param.25) | copy-start | bytes 24580
  6.5 11.1 %copy-start.39 = (f32[2,1024]{1,0:T(2,128)S(1)}, f32[2,1024]{1,0:T(2,128)}, u32[]{:S(2)}) copy-start(f32[2,1024]{1,0:T(2,128)} %param.26) | copy-start | bytes 24580
  6.5 11.7 %copy-start.16 = (f32[2,4,1024]{2,1,0:T(4,128)S(1)}, f32[2,4,1024]{2,1,0:T(4,128)}, u32[]{:S(2)}) copy-start(f32[2,4,1024]{2,1,0:T(4,128)} %param.20) | copy-start | bytes 98308
  6.6 12.3 %copy-start.17 = (f32[2,4096]{1,0:T(2,128)S(1)}, f32[2,4096]{1,0:T(2,128)}, u32[]{:S(2)}) copy-start(f32[2,4096]{1,0:T(2,128)} %param.18) | copy-start | bytes 98308
  6.6 197.4 %all-gather.7.cloned.1.call-start = ((), (), s32[]{:S(2)}) async-start(), calls=%async_computation | async-start | bytes 17825792 | tf_op jit(solution)/shard_map/all_gather | solution.py:61
  7.3 438.5 %all-gather.9.cloned.1.call-start = ((), (), s32[]{:S(2)}) async-start(), calls=%async_computation.1 | async-start | bytes 17825792 | tf_op jit(solution)/shard_map/all_gather | solution.py:62
  8.1 467.1 %all-reduce.67.cloned.1.call-start = ((), (), s32[]{:S(2)}) async-start(), calls=%async_computation.2 | async-start | bytes 4194304 | tf_op jit(solution)/shard_map/psum | solution.py:108
  8.9 10.7 %collective-permute-start.1 = (bf16[3]{0:T(256)(128)(2,1)S(1)}, bf16[3]{0:T(256)(128)(2,1)S(1)}, u32[]{:S(2)}, u32[]{:S(2)}) collective-permute-start(bf16[3]{0:T(256)(128)(2,1)S(1)} %slice.605), channel_id=1, source_target_pairs={{0,2},{2,4},{4,6},{6,8},{8,10},{10,12},{12,14},{14,16},{16,18},{18... | collective-permute-start | bytes 26 | tf_op jit(solution)/shard_map/ppermute | solution.py:13
  204.0 8.8 %copy-start.42 = (s32[256]{0:T(256)S(1)}, s32[256]{0:T(256)}, u32[]{:S(2)}) copy-start(s32[256]{0:T(256)} %param.17) | copy-start | bytes 3076
  209.8 4.3 collective-permute-start
  212.8 14.9 %copy-start.30 = (pred[256]{0:T(512)(128)(4,1)}, pred[256]{0:T(512)(128)(4,1)S(1)}, u32[]{:S(2)}) copy-start(pred[256]{0:T(512)(128)(4,1)S(1)} %get-tuple-element.209) | copy-start | bytes 772
  212.9 14.9 %copy-start.32 = (pred[256]{0:T(512)(128)(4,1)}, pred[256]{0:T(512)(128)(4,1)S(1)}, u32[]{:S(2)}) copy-start(pred[256]{0:T(512)(128)(4,1)S(1)} %get-tuple-element.211) | copy-start | bytes 772
  212.9 14.9 %copy-start.34 = (pred[256]{0:T(512)(128)(4,1)}, pred[256]{0:T(512)(128)(4,1)S(1)}, u32[]{:S(2)}) copy-start(pred[256]{0:T(512)(128)(4,1)S(1)} %get-tuple-element.212) | copy-start | bytes 772
  212.9 14.9 %copy-start.40 = (pred[256]{0:T(512)(128)(4,1)}, pred[256]{0:T(512)(128)(4,1)S(1)}, u32[]{:S(2)}) copy-start(pred[256]{0:T(512)(128)(4,1)S(1)} %get-tuple-element.210) | copy-start | bytes 772
  246.1 0.9 copy-start.5
  247.8 60.8 %copy-start.3 = (f32[256,1024]{1,0:T(8,128)S(1)}, f32[256,1024]{1,0:T(8,128)}, u32[]{:S(2)}) copy-start(f32[256,1024]{1,0:T(8,128)} %get-tuple-element.122) | copy-start | bytes 3145732
  302.4 21.8 %copy-start.9 = (f32[31,1024]{1,0:T(8,128)S(1)}, f32[31,1024]{1,0:T(8,128)}, u32[]{:S(2)}) copy-start(f32[31,1024]{1,0:T(8,128)} %slice.673) | copy-start | bytes 380932
  323.3 5.1 copy-start.21
  326.5 8.6 %copy-start.20 = (f32[1,1024]{1,0:T(1,128)S(1)}, f32[1,1024]{1,0:T(1,128)}, u32[]{:S(2)}) copy-start(f32[1,1024]{1,0:T(1,128)} %slice.823) | copy-start | bytes 12292
  335.1 10.6 %copy-start.19 = (f32[1,1024]{1,0:T(1,128)S(1)}, f32[1,1024]{1,0:T(1,128)}, u32[]{:S(2)}) copy-start(f32[1,1024]{1,0:T(1,128)} %slice.796) | copy-start | bytes 12292
  343.1 52.4 %copy-start.18 = (f32[1,1024]{1,0:T(1,128)S(1)}, f32[1,1024]{1,0:T(1,128)}, u32[]{:S(2)}) copy-start(f32[1,1024]{1,0:T(1,128)} %slice.822) | copy-start | bytes 12292
  345.7 49.8 %copy-start.6 = (f32[127,1024]{1,0:T(8,128)S(1)}, f32[127,1024]{1,0:T(8,128)}, u32[]{:S(2)}) copy-start(f32[127,1024]{1,0:T(8,128)} %get-tuple-element.128) | copy-start | bytes 1560580
  454.3 23.3 %copy-start.29 = (f32[1,4096]{1,0:T(1,128)S(1)}, f32[1,4096]{1,0:T(1,128)}, u32[]{:S(2)}) copy-start(f32[1,4096]{1,0:T(1,128)} %get-tuple-element.172) | copy-start | bytes 49156
  454.4 289.2 %all-reduce.69.cloned.1.call-start = ((), (), s32[]{:S(2)}) async-start(), calls=%async_computation.3 | async-start | bytes 4194304 | tf_op jit(solution)/shard_map/psum | solution.py:108
  475.1 2.5 copy-start.1
  477.7 12.9 %copy-start.11 = (f32[1,1,1024]{2,1,0:T(1,128)S(1)}, f32[1,1,1024]{2,1,0:T(1,128)}, u32[]{:S(2)}) copy-start(f32[1,1,1024]{2,1,0:T(1,128)} %get-tuple-element.159) | copy-start | bytes 12292
  477.7 12.9 %copy-start.12 = (f32[1,1,1024]{2,1,0:T(1,128)S(1)}, f32[1,1,1024]{2,1,0:T(1,128)}, u32[]{:S(2)}) copy-start(f32[1,1,1024]{2,1,0:T(1,128)} %get-tuple-element.160) | copy-start | bytes 12292
  477.7 12.9 %copy-start.13 = (f32[1,1,1024]{2,1,0:T(1,128)S(1)}, f32[1,1,1024]{2,1,0:T(1,128)}, u32[]{:S(2)}) copy-start(f32[1,1,1024]{2,1,0:T(1,128)} %get-tuple-element.165) | copy-start | bytes 12292
  477.7 12.9 %copy-start.14 = (f32[1,1,1024]{2,1,0:T(1,128)S(1)}, f32[1,1,1024]{2,1,0:T(1,128)}, u32[]{:S(2)}) copy-start(f32[1,1,1024]{2,1,0:T(1,128)} %get-tuple-element.166) | copy-start | bytes 12292
  477.7 12.9 %copy-start.15 = (f32[1,1024]{1,0:T(1,128)S(1)}, f32[1,1024]{1,0:T(1,128)}, u32[]{:S(2)}) copy-start(f32[1,1024]{1,0:T(1,128)} %get-tuple-element.201) | copy-start | bytes 12292
  477.7 12.9 %copy-start.31 = (pred[256]{0:T(512)(128)(4,1)S(1)}, pred[256]{0:T(512)(128)(4,1)}, u32[]{:S(2)}) copy-start(pred[256]{0:T(512)(128)(4,1)} %copy-done.30) | copy-start | bytes 772
  477.7 12.9 %copy-start.33 = (pred[256]{0:T(512)(128)(4,1)S(1)}, pred[256]{0:T(512)(128)(4,1)}, u32[]{:S(2)}) copy-start(pred[256]{0:T(512)(128)(4,1)} %copy-done.32) | copy-start | bytes 772
  477.7 12.9 %copy-start.35 = (pred[256]{0:T(512)(128)(4,1)S(1)}, pred[256]{0:T(512)(128)(4,1)}, u32[]{:S(2)}) copy-start(pred[256]{0:T(512)(128)(4,1)} %copy-done.34) | copy-start | bytes 772
  483.5 0.8 copy-start.8
  484.4 5.0 collective-permute-start.2
  494.1 10.0 %copy-start.26 = (f32[1,1024]{1,0:T(1,128)S(1)}, f32[1,1024]{1,0:T(1,128)}, u32[]{:S(2)}) copy-start(f32[1,1024]{1,0:T(1,128)} %get-tuple-element.199) | copy-start | bytes 12292
  494.1 10.0 %copy-start.27 = (f32[1,1024]{1,0:T(1,128)S(1)}, f32[1,1024]{1,0:T(1,128)}, u32[]{:S(2)}) copy-start(f32[1,1024]{1,0:T(1,128)} %get-tuple-element.195) | copy-start | bytes 12292
  494.1 10.0 %copy-start.28 = (f32[1,1024]{1,0:T(1,128)S(1)}, f32[1,1024]{1,0:T(1,128)}, u32[]{:S(2)}) copy-start(f32[1,1024]{1,0:T(1,128)} %get-tuple-element.197) | copy-start | bytes 12292
  494.1 10.0 %copy-start.41 = (pred[256]{0:T(512)(128)(4,1)S(1)}, pred[256]{0:T(512)(128)(4,1)}, u32[]{:S(2)}) copy-start(pred[256]{0:T(512)(128)(4,1)} %copy-done.40) | copy-start | bytes 772
  522.5 1.6 copy-start.4
  524.2 63.4 %copy-start.2 = (f32[256,1024]{1,0:T(8,128)S(1)}, f32[256,1024]{1,0:T(8,128)}, u32[]{:S(2)}) copy-start(f32[256,1024]{1,0:T(8,128)} %get-tuple-element.120) | copy-start | bytes 3145732
  581.4 22.8 %copy-start.10 = (f32[31,1024]{1,0:T(8,128)S(1)}, f32[31,1024]{1,0:T(8,128)}, u32[]{:S(2)}) copy-start(f32[31,1024]{1,0:T(8,128)} %slice.767) | copy-start | bytes 380932
  603.4 5.0 copy-start.25
  606.6 8.5 %copy-start.24 = (f32[1,1024]{1,0:T(1,128)S(1)}, f32[1,1024]{1,0:T(1,128)}, u32[]{:S(2)}) copy-start(f32[1,1024]{1,0:T(1,128)} %slice.882) | copy-start | bytes 12292
  615.0 10.6 %copy-start.23 = (f32[1,1024]{1,0:T(1,128)S(1)}, f32[1,1024]{1,0:T(1,128)}, u32[]{:S(2)}) copy-start(f32[1,1024]{1,0:T(1,128)} %slice.855) | copy-start | bytes 12292
  623.0 52.6 %copy-start.22 = (f32[1,1024]{1,0:T(1,128)S(1)}, f32[1,1024]{1,0:T(1,128)}, u32[]{:S(2)}) copy-start(f32[1,1024]{1,0:T(1,128)} %slice.881) | copy-start | bytes 12292
  625.6 50.0 %copy-start.7 = (f32[127,1024]{1,0:T(8,128)S(1)}, f32[127,1024]{1,0:T(8,128)}, u32[]{:S(2)}) copy-start(f32[127,1024]{1,0:T(8,128)} %get-tuple-element.124) | copy-start | bytes 1560580
Sparse Core Ops, SparseCore 0:
  10.1 193.7 all-gather.6
  206.7 233.8 all-gather.8
  454.5 20.5 all-reduce.66
  723.5 19.9 all-reduce.68
where the time goes:
time: 762 us; the launch traced here: 755 us
  waiting for transfers between devices  229 us (30%)
  local copies, waits for them, and re-layouts  206 us (27%)
  blocking collectives  166 us (22%)
  other arithmetic  89.8 us (12%)
  matrix products  38.3 us (5%)
  between operations  14.2 us (2%)
  starting transfers between devices  11.6 us (2%)
    all_gather x1, waiting for transfers between devices, per_device(): lax.all_gather(in_weight, 'sp', axis=1, tiled=True)  184 us
    all_gather x4, blocking collectives, carried_in(): gathered = jax.tree.map(lambda a: lax.all_gather(a, axis), part)  166 us
    slice x104, local copies, waits for them, and re-layouts, per_device(): lax.associative_scan(combine, (decay_now, drive_term), axis=0)  145 us
    pad x56, local copies, waits for them, and re-layouts, per_device(): lax.associative_scan(combine, (decay_now, drive_term), axis=0)  42.5 us
    psum x2, waiting for transfers between devices, per_device(): lax.psum(partial_sum.astype(jnp.bfloat16), 'tp').astype(jnp.float32)  40.8 us
    add x26, other arithmetic, combine(): return (earlier[0] * following[0], following[0] * earlier[1] + following[1])  36.2 us
    dot_general x2, matrix products, per_device(): jnp.dot(hidden, whole_out[depth_at], preferred_element_type=jnp.float32)  16.9 us
    concatenate x27, other arithmetic, per_device(): lax.associative_scan(combine, (decay_now, drive_term), axis=0)  16 us
  transfers between devices with their start and end apart: 7, of which 5 were waited for; matrix products, arithmetic and copies ran while one was open for 21% of the time, Pallas kernels for 0%

commit v1 on v0

v1 whole, which is shorter than its diff:
```python
import functools

import jax
import jax.numpy as jnp
from jax import lax
from jax.experimental import pallas as pl
from jax.experimental.pallas import tpu as pltpu
from jax.sharding import PartitionSpec as P

RG_C = 8.0
EPS = 0.1
MESH = pl.DeviceIdType.MESH
F32 = jnp.float32
BF16 = jnp.bfloat16
VM = pl.BlockSpec(memory_space=pltpu.VMEM)


def send(src, dst, send_sem, recv_sem, **device):
    return pltpu.make_async_remote_copy(
        src_ref=src,
        dst_ref=dst,
        send_sem=send_sem,
        recv_sem=recv_sem,
        device_id=device,
        device_id_type=MESH,
    )


def swap_kernel(g, x_ref, o_ref, send_sem, recv_sem, own_sem):
    me = lax.axis_index("sp")
    inner, base = lax.rem(me, g), me - lax.rem(me, g)
    own = pltpu.make_async_copy(x_ref.at[inner], o_ref.at[inner], own_sem)
    own.start()

    def go(step, _):
        j = lax.rem(inner + step, g)
        send(x_ref.at[j], o_ref.at[inner], send_sem.at[j], recv_sem.at[inner], sp=base + j).start()
        return 0

    lax.fori_loop(1, g, go, 0)

    def done(step, _):
        j = lax.rem(inner + step, g)
        copy = send(x_ref.at[j], o_ref.at[j], send_sem.at[j], recv_sem.at[j], sp=base + j)
        copy.wait_recv()
        copy.wait_send()
        return 0

    lax.fori_loop(1, g, done, 0)
    own.wait()


def swapped(x, g):
    return pl.pallas_call(
        functools.partial(swap_kernel, g),
        out_shape=jax.ShapeDtypeStruct(x.shape, x.dtype),
        in_specs=[pl.BlockSpec(memory_space=pl.ANY)],
        out_specs=pl.BlockSpec(memory_space=pl.ANY),
        scratch_shapes=[
            pltpu.SemaphoreType.DMA((g,)),
            pltpu.SemaphoreType.DMA((g,)),
            pltpu.SemaphoreType.DMA,
        ],
        compiler_params=pltpu.CompilerParams(has_side_effects=True),
    )(x)


def minus_expm1(x):
    series = 1.0 + x * (1.0 / 8.0)
    for n in range(7, 1, -1):
        series = 1.0 + (x * (1.0 / n)) * series
    return jnp.where(x > -0.5, -x * series, 1.0 - jnp.exp(x))


def layer_kernel(
    g, n_sp, n_tp, taps, feature_count,
    x_ref, gain_ref, win_ref, wout_ref, vec_ref, mask_ref, gate_ref,
    o_ref,
    part, gotten, tails, tail_out, ext, a_buf, b_buf, ends, hid, psend, pgot,
    rs_send, rs_recv, tail_sem, end_send, end_recv, ag_send, ag_recv, tp_send, tp_recv,
):
    me = lax.axis_index("sp")
    core = lax.axis_index("tp")
    inner, base = lax.rem(me, g), me - lax.rem(me, g)
    rows = x_ref.shape[1]
    chans = win_ref.shape[1]
    sub = rows // 8

    def project(step, _):
        j = lax.rem(inner + step, g)
        x = x_ref[j].astype(F32)
        squares = jnp.sum(x * x, axis=1, keepdims=True)
        high = squares.astype(BF16).astype(F32)
        lane = lax.broadcasted_iota(jnp.int32, (rows, 128), 1)
        extra = jnp.where(lane == 0, high, jnp.where(lane == 1, squares - high, 0.0))
        scaled = (x * gain_ref[...]).astype(BF16)
        out = jnp.dot(scaled, win_ref[...], preferred_element_type=F32)
        part[j, :, :chans] = out.astype(BF16)
        part[j, :, chans:] = extra.astype(BF16)

        @pl.when(step < g)
        def _():
            send(
                part.at[j], gotten.at[inner], rs_send.at[j], rs_recv.at[inner], sp=base + j
            ).start()

        return 0

    lax.fori_loop(1, g + 1, project, 0)
    ext[pl.ds(8, rows), :] = part[inner, :, :chans].astype(F32)
    sums = part[inner, :, chans:].astype(F32)

    def collect(step, sums):
        j = lax.rem(inner + step, g)
        send(part.at[j], gotten.at[j], rs_send.at[j], rs_recv.at[j], sp=base + j).wait_recv()
        ext[pl.ds(8, rows), :] += gotten[j, :, :chans].astype(F32)
        return sums + gotten[j, :, chans:].astype(F32)

    sums = lax.fori_loop(1, g, collect, sums)
    total = jnp.sum(sums, axis=1, keepdims=True)
    scale = lax.rsqrt(total * (1.0 / feature_count) + EPS)
    mixed = (ext[pl.ds(8, rows), :] * scale).astype(BF16)
    tail_out[...] = mixed[rows - 16 :]

    after = lax.rem(me + 1, n_sp)

    tail_copy = send(tail_out, tails, tail_sem.at[0], tail_sem.at[1], sp=after)

    tail_copy.start()
    ext[pl.ds(8, rows), :] = mixed.astype(F32)
    tail_copy.wait_recv()
    ext[pl.ds(0, 8), :] = tails[8:].astype(F32)

    pair = gate_ref.shape[1]
    for col in range(0, chans, pair):
        cols = pl.ds(col, pair)
        conv = vec_ref[pl.ds(taps, 1), cols] + vec_ref[pl.ds(0, 1), cols] * ext[pl.ds(8, rows), cols]
        for lag in range(1, taps):
            shifted = ext[pl.ds(8 - lag, rows), cols]
            same = mask_ref[:, lag : lag + 1] > 0.5
            conv = conv + jnp.where(same, vec_ref[pl.ds(lag, 1), cols] * shifted, 0.0)
        conv_out = conv.astype(BF16)
        both = jnp.dot(conv_out, gate_ref[col // pair], preferred_element_type=F32)
        recur = jax.nn.sigmoid(both[:, :pair] + vec_ref[pl.ds(taps + 1, 1), cols])
        inp = jax.nn.sigmoid(both[:, pair:] + vec_ref[pl.ds(taps + 2, 1), cols])
        log_decay = vec_ref[pl.ds(taps + 3, 1), cols] * recur
        keep = mask_ref[:, 0:1] > 0.5
        a_buf[col // pair] = jnp.where(keep, jnp.exp(log_decay), 0.0)
        b_buf[col // pair] = jnp.sqrt(jnp.maximum(minus_expm1(2.0 * log_decay), 0.0)) * (
            inp * conv_out.astype(F32)
        )

    lanes = a_buf.shape[0]

    def advance(r, carry):
        at = pl.ds(r, 8, stride=sub)
        following = []
        for c in range(lanes):
            decay, state = carry[c]
            a = a_buf[c, at, :]
            decay = decay * a
            state = a * state + b_buf[c, at, :]
            a_buf[c, at, :] = decay
            b_buf[c, at, :] = state
            following.append((decay, state))
        return tuple(following)

    start = (jnp.ones((8, pair), F32), jnp.zeros((8, pair), F32))
    chunks = lax.fori_loop(0, sub, advance, (start,) * lanes, unroll=2)
    decay = jnp.concatenate([c[0] for c in chunks], axis=1)
    state = jnp.concatenate([c[1] for c in chunks], axis=1)
    prefix = [(jnp.ones((1, chans), F32), jnp.zeros((1, chans), F32))]
    for s in range(8):
        d, h = prefix[-1]
        prefix.append((d * decay[s : s + 1], decay[s : s + 1] * h + state[s : s + 1]))
    ends[me, 0:1, :] = prefix[8][0]
    ends[me, 1:2, :] = prefix[8][1]

    def end_to(dst, _):
        @pl.when(dst > me)
        def _():
            send(ends.at[me], ends.at[me], end_send.at[dst], end_recv.at[me], sp=dst).start()

        return 0

    lax.fori_loop(0, n_sp, end_to, 0)

    def fold(src, state):
        @pl.when(src < me)
        def _():
            send(ends.at[src], ends.at[src], end_send.at[src], end_recv.at[src], sp=src).wait_recv()

        return jnp.where(src < me, ends[src, 0:1, :] * state + ends[src, 1:2, :], state)

    carried = lax.fori_loop(0, n_sp, fold, jnp.zeros((1, chans), F32))
    for s in range(8):
        at = pl.ds(s * sub, sub)
        enter = prefix[s][0] * carried + prefix[s][1]
        for c in range(lanes):
            cols = pl.ds(c * pair, pair)
            one = enter[:, c * pair : (c + 1) * pair]
            hid[inner, at, cols] = (b_buf[c, at, :] + a_buf[c, at, :] * one).astype(BF16)

    def spread(step, _):
        j = lax.rem(inner + step, g)
        send(hid.at[inner], hid.at[inner], ag_send.at[j], ag_recv.at[inner], sp=base + j).start()
        return 0

    lax.fori_loop(1, g, spread, 0)

    blocks, width = wout_ref.shape[0], wout_ref.shape[2]

    def unproject(step, _):
        j = lax.rem(inner + step, g)

        @pl.when(step > 0)
        def _():
            send(hid.at[j], hid.at[j], ag_send.at[j], ag_recv.at[j], sp=base + j).wait_recv()

        h = hid[j]
        for block in range(blocks):
            out = jnp.dot(h, wout_ref[block], preferred_element_type=F32)
            psend[j, :, block * width : (block + 1) * width] = out.astype(BF16)
        for other in range(1, n_tp):
            peer = lax.rem(core + other, n_tp)
            send(
                psend.at[j], pgot.at[core, j], tp_send.at[peer, j], tp_recv.at[core, j], tp=peer
            ).start()
        return 0

    lax.fori_loop(0, g, unproject, 0)

    def finish(step, _):
        j = lax.rem(inner + step, g)
        summed = psend[j].astype(F32)
        for other in range(1, n_tp):
            peer = lax.rem(core + other, n_tp)
            copy = send(
                psend.at[j], pgot.at[peer, j], tp_send.at[peer, j], tp_recv.at[peer, j], tp=peer
            )
            copy.wait_recv()
            summed = summed + pgot[peer, j].astype(F32)
            copy.wait_send()
        o_ref[j] = (x_ref[j].astype(F32) + summed).astype(BF16)
        return 0

    lax.fori_loop(0, g, finish, 0)

    def close(step, _):
        j = lax.rem(inner + step, g)
        send(part.at[j], gotten.at[j], rs_send.at[j], rs_recv.at[j], sp=base + j).wait_send()
        send(hid.at[inner], hid.at[j], ag_send.at[j], ag_recv.at[j], sp=base + j).wait_send()
        return 0

    lax.fori_loop(1, g, close, 0)
    tail_copy.wait_send()

    def end_close(dst, _):
        @pl.when(dst > me)
        def _():
            send(ends.at[me], ends.at[me], end_send.at[dst], end_recv.at[me], sp=dst).wait_send()

        return 0

    lax.fori_loop(0, n_sp, end_close, 0)


def one_layer(g, n_sp, n_tp, taps, x, gain, win, wout, vec, mask, gates, features):
    rows, part_width = x.shape[1], x.shape[2]
    chans = win.shape[1]
    dma = pltpu.SemaphoreType.DMA
    return pl.pallas_call(
        functools.partial(layer_kernel, g, n_sp, n_tp, taps, features),
        out_shape=jax.ShapeDtypeStruct(x.shape, x.dtype),
        in_specs=[VM] * 7,
        out_specs=VM,
        scratch_shapes=[
            pltpu.VMEM((g, rows, chans + 128), BF16),
            pltpu.VMEM((g, rows, chans + 128), BF16),
            pltpu.VMEM((16, chans), BF16),
            pltpu.VMEM((16, chans), BF16),
            pltpu.VMEM((rows + 8, chans), F32),
            pltpu.VMEM((chans // 128, rows, 128), F32),
            pltpu.VMEM((chans // 128, rows, 128), F32),
            pltpu.VMEM((n_sp, 2, chans), F32),
            pltpu.VMEM((g, rows, chans), BF16),
            pltpu.VMEM((g, rows, part_width), BF16),
            pltpu.VMEM((n_tp, g, rows, part_width), BF16),
            dma((g,)),
            dma((g,)),
            dma((2,)),
            dma((n_sp,)),
            dma((n_sp,)),
            dma((g,)),
            dma((g,)),
            dma((n_tp, g)),
            dma((n_tp, g)),
        ],
        compiler_params=pltpu.CompilerParams(
            has_side_effects=True, vmem_limit_bytes=60 * 1024 * 1024
        ),
        cost_estimate=pl.CostEstimate(
            flops=100_000_000_000, bytes_accessed=100_000_000, transcendentals=0
        ),
    )(x, gain, win, wout, vec, mask, gates)


def per_device(
    g,
    tokens,
    documents,
    norm_gain,
    in_weight,
    conv_taps,
    conv_bias,
    recur_gate,
    input_gate,
    recur_bias,
    input_bias,
    decay_param,
    out_weight,
):
    n_sp, n_tp = lax.axis_size("sp"), lax.axis_size("tp")
    outer = n_sp // g
    rows, features = tokens.shape
    layers, block_width, chans = in_weight.shape
    taps = conv_taps.shape[1]
    me = lax.axis_index("sp")
    inner = lax.rem(me, g)
    groups = [[o * g + i for o in range(outer)] for i in range(g)]

    wins, wouts = [], []
    for l in range(layers):
        wins.append(
            lax.all_gather(in_weight[l], "sp", axis=0, tiled=True, axis_index_groups=groups)
        )
        wouts.append(lax.all_gather(out_weight[l], "sp", axis=0, axis_index_groups=groups))

    head = taps - 1
    tail_doc = lax.ppermute(
        documents[rows - head :], "sp", [(i, i + 1) for i in range(n_sp - 1)]
    )
    tail_doc = jnp.where(me == 0, -1, tail_doc)
    ext_doc = jnp.concatenate([tail_doc, documents])
    same = [ext_doc[head - lag : head - lag + rows] == documents for lag in range(1, taps)]
    mask = jnp.stack([same[0]] + same, axis=1).astype(F32)
    mask = jnp.pad(mask, ((0, 0), (0, 128 - mask.shape[1])))

    def paired(w):
        blocks, dim = w.shape[1], w.shape[2]
        per = 128 // dim
        w = w.reshape(layers, blocks // per, per, dim, dim)
        eye = jnp.eye(per, dtype=w.dtype)
        full = w[:, :, :, :, None, :] * eye[None, None, :, None, :, None]
        return full.reshape(layers, blocks // per, per * dim, per * dim)

    gates = jnp.concatenate([paired(recur_gate), paired(input_gate)], axis=3)
    coef = -RG_C * jax.nn.softplus(-decay_param)
    vec = jnp.concatenate(
        [
            conv_taps,
            conv_bias[:, None],
            recur_bias[:, None],
            input_bias[:, None],
            coef[:, None],
        ],
        axis=1,
    )
    gain = lax.dynamic_index_in_dim(
        norm_gain.reshape(layers, outer, g, block_width), inner, 2, False
    ).reshape(layers, 1, outer * block_width)

    x = tokens.reshape(rows, outer, g, block_width).transpose(2, 0, 1, 3)
    x = swapped(x.reshape(g, rows, outer * block_width), g)
    for l in range(layers):
        x = one_layer(
            g, n_sp, n_tp, taps, x, gain[l], wins[l], wouts[l], vec[l], mask, gates[l], features
        )
    x = swapped(x, g)
    x = x.reshape(g, rows, outer, block_width).transpose(1, 2, 0, 3)
    return x.reshape(rows, features)


def solution(mesh):
    n_sp = mesh.shape["sp"]
    g = 4 if n_sp % 4 == 0 else 1
    return jax.shard_map(
        functools.partial(per_device, g),
        mesh=mesh,
        in_specs=(
            P("sp", None),
            P("sp"),
            P(),
            P(None, "sp", "tp"),
            P(None, None, "tp"),
            P(None, "tp"),
            P(None, "tp", None, None),
            P(None, "tp", None, None),
            P(None, "tp"),
            P(None, "tp"),
            P(None, "tp"),
            P(None, "tp", "sp"),
        ),
        out_specs=P("sp", None),
        check_vma=False,
    )
```

time: 762 us -> 325 us (0.43)
  Pallas kernels: 0 us -> 221 us
  waiting for transfers between devices: 229 us -> 52.9 us
  local copies, waits for them, and re-layouts: 206 us -> 30.4 us
  blocking collectives: 166 us -> 0 us
  other arithmetic: 89.8 us -> 2.06 us
  matrix products: 38.3 us -> 0 us
    pallas_call x0 -> x4, Pallas kernels: none -> 221 us  [the longest x2 159 us: one_layer(): pl.pallas_call(functools.partial(layer_kernel, g, n_sp, n_tp, taps, featu...]
    all_gather x4 -> x0, blocking collectives: 166 us -> none  [carried_in(): gathered = jax.tree.map(lambda a: lax.all_gather(a, axis), part)]
    slice x112 -> x4, local copies, waits for them, and re-layouts: 148 us -> 4.08 us  [the longest x1 2.38 us: per_device(): out_weight[l]]
    all_gather x2 -> x4, waiting for transfers between devices: 184 us -> 52.2 us  [the longest x2 52.2 us: per_device(): lax.all_gather(in_weight[l], 'sp', axis=0, tiled=True, axis_index_groups=...]
    add x53 -> x0, other arithmetic: 45 us -> none  [the longest x26 36.2 us: combine(): return (earlier[0] * following[0], following[0] * earlier[1] + following[1])]
    pad x56 -> x0, local copies, waits for them, and re-layouts: 42.5 us -> none  [per_device(): lax.associative_scan(combine, (decay_now, drive_term), axis=0)]
    psum x2 -> x0, waiting for transfers between devices: 40.8 us -> none  [per_device(): lax.psum(partial_sum.astype(jnp.bfloat16), 'tp').astype(jnp.float32)]
    dot_general x8 -> x0, matrix products: 38.3 us -> none  [the longest x2 16.9 us: per_device(): jnp.dot(hidden, whole_out[depth_at], preferred_element_type=jnp.float32)]
  transfers between devices with their start and end apart: 7 -> 5, of which waited for: 5 -> 2; matrix products, arithmetic and copies ran while one was open for 21% -> 6% of each run, Pallas kernels for 0% -> 34%
where the time goes in v1:
time: 325 us
  Pallas kernels  221 us (68%)
  waiting for transfers between devices  52.9 us (16%)
  local copies, waits for them, and re-layouts  30.4 us (9%)
  between operations  13.5 us (4%)
  starting transfers between devices  4.98 us (2%)
    pallas_call x2, Pallas kernels, one_layer(): pl.pallas_call(functools.partial(layer_kernel, g, n_sp, n_tp, taps, featu...  159 us
    pallas_call x2, Pallas kernels, swapped(): pl.pallas_call(functools.partial(swap_kernel, g), out_shape=jax.ShapeDtyp...  61.8 us
    all_gather x2, waiting for transfers between devices, per_device(): lax.all_gather(in_weight[l], 'sp', axis=0, tiled=True, axis_index_groups=...  52.2 us
  transfers between devices with their start and end apart: 5, of which 2 were waited for; matrix products, arithmetic and copies ran while one was open for 6% of the time, Pallas kernels for 34%

profile of v1, /device:TPU:0, one launch (start us, length us, event | category | flops | bytes accessed | tf_op | source)
XLA Modules:
  0.0 325.1 jit_solution(15809211913464516527)
XLA Ops:
  6.5 0.0 copy-start.3
  6.5 0.0 all-gather.7.cloned.1.call-start
  6.5 2.4 fusion.4
  8.9 0.0 copy-start.11
  8.9 0.0 copy-start.5
  8.9 0.0 copy-start.4
  8.9 0.0 all-gather.7.cloned.1.call-update
  9.0 0.0 all-gather.11.cloned.1.call-start
  9.0 0.0 copy-done.3
  9.0 1.0 fusion.5
  10.0 0.0 all-gather.11.cloned.1.call-update
  10.1 0.0 all-gather.9.cloned.1.call-start
  10.1 0.7 all-gather.9.cloned.1.call-update
  10.8 0.0 all-gather.13.cloned.1.call-start
  10.9 0.0 copy-done.11
  10.9 0.1 slice.48
  10.9 4.9 %collective-permute-start = (s32[3]{0:T(128)S(1)}, s32[3]{0:T(128)S(1)}, u32[]{:S(2)}, u32[]{:S(2)}) collective-permute-start(s32[3]{0:T(128)S(1)} %slice.48), channel_id=1, source_target_pairs={{0,2},{2,4},{4,6},{6,8},{8,10},{10,12},{12,14},{14,16},{16,18},{18... | collective-permute-start | bytes 44 | tf_op jit(solution)/shard_map/ppermute | solution.py:340
  15.8 0.0 all-gather.13.cloned.1.call-update
  15.9 0.0 copy-done.5
  15.9 0.0 copy-done.4
  15.9 0.8 mul.53
  16.7 0.0 copy-start.7
  16.7 0.0 copy-start.8
  16.7 0.0 copy-start.9
  16.7 0.0 copy-start.10
  16.8 0.0 copy-start.6
  16.8 1.3 mul.54
  18.1 0.0 copy-start
  18.1 2.0 mul.60
  20.1 1.3 mul.61
  21.4 0.1 mul.55
  21.5 0.1 mul.56
  21.6 0.0 copy-done.7
  21.7 0.0 copy-done.8
  21.7 0.0 copy-done.9
  21.7 0.0 copy-done.10
  21.7 0.0 copy-done.6
  21.7 0.1 concatenate.9
  21.8 0.6 slice_bitcast_fusion
  22.5 0.0 copy-done
  22.5 2.7 reshape.37
  25.2 2.4 copy.31
  27.6 2.7 reshape.38.x_ref
  30.3 0.0 copy-start.2
  30.3 30.5 %shard_map.118.x_ref = bf16[4,256,1024]{2,1,0:T(8,128)(2,1)} custom-call(bf16[4,256,1024]{2,1,0:T(8,128)(2,1)} %reshape.38.x_ref), custom_call_target="tpu_custom_call" | custom-call | tf_op jit(solution)/shard_map/pallas_call | solution.py:54
  60.8 0.0 copy-done.1
  60.8 0.0 copy-done.2
  60.8 0.1 broadcast_multiply_fusion
  60.9 1.1 fusion.2
  62.0 0.6 constant_dynamic-slice_fusion.1
  62.6 0.0 collective-permute-done
  62.6 0.1 pad_add_fusion.1
  62.7 0.1 slice_compare_fusion.2
  62.8 0.2 copy.25
  63.0 0.7 pad_convert_fusion.mask_ref
  63.7 39.9 %all-gather.11.cloned.1.call-done = bf16[1,1024,1024]{2,1,0:T(8,128)(2,1)} async-done(((bf16[1,256,1024]{2,1,0:T(8,128)(2,1)}), bf16[1,1024,1024]{2,1,0:T(8,128)(2,1)}) %all-gather.11.cloned.1.call-update) | async-done | bytes 2097168 | tf_op jit(solution)/shard_map/all_gather | solution.py:335
  103.5 80.3 %shard_map.119.x_ref = bf16[4,256,1024]{2,1,0:T(8,128)(2,1)} custom-call(bf16[4,256,1024]{2,1,0:T(8,128)(2,1)} %shard_map.118.x_ref, f32[1,1024]{1,0:T(1,128)} %bitcast.23, bf16[1024,1024]{1,0:T(8,128)(2,1)} %bitcast.24, bf16[4,1024,256]{2,1,0:T(8,128)(2,1)} %all-gather.7.cloned.1.call-done.wout_ref, f32[8,1024]{1,0:T(8,128)} %get-tuple-element.12.vec_ref, ...), custom_call_target="tpu_custom_call" | custom-call | flops 99999997952 | bytes 100000000 | tf_op jit(solution)/shard_map/pallas_call | solution.py:272
  183.9 0.0 all-gather.9.cloned.1.call-done.wout_ref
  183.9 12.3 %all-gather.13.cloned.1.call-done = bf16[1,1024,1024]{2,1,0:T(8,128)(2,1)} async-done(((bf16[1,256,1024]{2,1,0:T(8,128)(2,1)}), bf16[1,1024,1024]{2,1,0:T(8,128)(2,1)}) %all-gather.13.cloned.1.call-update) | async-done | bytes 2097168 | tf_op jit(solution)/shard_map/all_gather | solution.py:335
  196.2 79.1 %shard_map.120.x_ref = bf16[4,256,1024]{2,1,0:T(8,128)(2,1)} custom-call(bf16[4,256,1024]{2,1,0:T(8,128)(2,1)} %shard_map.119.x_ref, f32[1,1024]{1,0:T(1,128)} %bitcast.22, bf16[1024,1024]{1,0:T(8,128)(2,1)} %bitcast.25, bf16[4,1024,256]{2,1,0:T(8,128)(2,1)} %all-gather.9.cloned.1.call-done.wout_ref, f32[8,1024]{1,0:T(8,128)} %get-tuple-element.11.vec_ref, ...), custom_call_target="tpu_custom_call" | custom-call | flops 99999997952 | bytes 100000000 | tf_op jit(solution)/shard_map/pallas_call | solution.py:272
  275.3 31.4 %shard_map.121 = bf16[4,256,1024]{2,1,0:T(8,128)(2,1)} custom-call(bf16[4,256,1024]{2,1,0:T(8,128)(2,1)} %shard_map.120.x_ref), custom_call_target="tpu_custom_call" | custom-call | tf_op jit(solution)/shard_map/pallas_call | solution.py:54
  306.7 3.3 %reshape.40 = bf16[4,256,4,256]{3,2,1,0:T(4,128)(2,1)S(1)} reshape(bf16[4,256,1024]{2,1,0:T(8,128)(2,1)} %shard_map.121) | data formatting | bytes 4194304 | tf_op jit(solution)/shard_map/reshape | solution.py:380
  310.1 4.0 %copy.26 = bf16[256,4,4,256]{3,2,1,0:T(4,128)(2,1)} copy(bf16[256,4,4,256]{3,1,0,2:T(4,128)(2,1)S(1)} %bitcast.19) | data formatting | bytes 4194304 | tf_op jit(solution)/shard_map/transpose | solution.py:380
  314.1 4.4 %reshape.41 = bf16[256,4096]{1,0:T(8,128)(2,1)} reshape(bf16[256,4,4,256]{3,2,1,0:T(4,128)(2,1)} %copy.26) | data formatting | bytes 4194304 | tf_op jit(solution)/shard_map/reshape | solution.py:381
  (14 shorter events, 0.1 us)
Async XLA Ops:
  6.5 2.5 copy-start.3
  6.5 57.1 %all-gather.7.cloned.1.call-start = ((), (), s32[]{:S(2)}) async-start(), calls=%async_computation | async-start | bytes 2621440 | tf_op jit(solution)/shard_map/all_gather | solution.py:337
  8.9 1.9 copy-start.11
  8.9 6.9 %copy-start.5 = (f32[2,4096]{1,0:T(2,128)S(1)}, f32[2,4096]{1,0:T(2,128)}, u32[]{:S(2)}) copy-start(f32[2,4096]{1,0:T(2,128)} %param.14) | copy-start | bytes 98308
  8.9 7.0 %copy-start.4 = (bf16[2,16,64,64]{3,2,1,0:T(8,128)(2,1)S(1)}, bf16[2,16,64,64]{3,2,1,0:T(8,128)(2,1)}, u32[]{:S(2)}) copy-start(bf16[2,16,64,64]{3,2,1,0:T(8,128)(2,1)} %param.18) | copy-start | bytes 786436
  9.0 94.6 %all-gather.11.cloned.1.call-start = ((), (), s32[]{:S(2)}) async-start(), calls=%async_computation.2 | async-start | bytes 2621440 | tf_op jit(solution)/shard_map/all_gather | solution.py:335
  10.1 173.9 %all-gather.9.cloned.1.call-start = ((), (), s32[]{:S(2)}) async-start(), calls=%async_computation.1 | async-start | bytes 2621440 | tf_op jit(solution)/shard_map/all_gather | solution.py:337
  10.8 185.4 %all-gather.13.cloned.1.call-start = ((), (), s32[]{:S(2)}) async-start(), calls=%async_computation.3 | async-start | bytes 2621440 | tf_op jit(solution)/shard_map/all_gather | solution.py:335
  10.9 51.7 %collective-permute-start = (s32[3]{0:T(128)S(1)}, s32[3]{0:T(128)S(1)}, u32[]{:S(2)}, u32[]{:S(2)}) collective-permute-start(s32[3]{0:T(128)S(1)} %slice.48), channel_id=1, source_target_pairs={{0,2},{2,4},{4,6},{6,8},{8,10},{10,12},{12,14},{14,16},{16,18},{18... | collective-permute-start | bytes 44 | tf_op jit(solution)/shard_map/ppermute | solution.py:340
  16.7 4.9 %copy-start.7 = (f32[2,1024]{1,0:T(2,128)S(1)}, f32[2,1024]{1,0:T(2,128)}, u32[]{:S(2)}) copy-start(f32[2,1024]{1,0:T(2,128)} %param.22) | copy-start | bytes 24580
  16.7 4.9 %copy-start.8 = (f32[2,1024]{1,0:T(2,128)S(1)}, f32[2,1024]{1,0:T(2,128)}, u32[]{:S(2)}) copy-start(f32[2,1024]{1,0:T(2,128)} %param.17) | copy-start | bytes 24580
  16.7 5.0 %copy-start.9 = (f32[2,1024]{1,0:T(2,128)S(1)}, f32[2,1024]{1,0:T(2,128)}, u32[]{:S(2)}) copy-start(f32[2,1024]{1,0:T(2,128)} %param.20) | copy-start | bytes 24580
  16.7 5.0 %copy-start.10 = (f32[2,1024]{1,0:T(2,128)S(1)}, f32[2,1024]{1,0:T(2,128)}, u32[]{:S(2)}) copy-start(f32[2,1024]{1,0:T(2,128)} %param.21) | copy-start | bytes 24580
  16.8 5.0 %copy-start.6 = (f32[2,4,1024]{2,1,0:T(4,128)S(1)}, f32[2,4,1024]{2,1,0:T(4,128)}, u32[]{:S(2)}) copy-start(f32[2,4,1024]{2,1,0:T(4,128)} %param.16) | copy-start | bytes 98308
  18.1 4.4 %copy-start = (bf16[256,4096]{1,0:T(8,128)(2,1)S(1)}, bf16[256,4096]{1,0:T(8,128)(2,1)}, u32[]{:S(2)}) copy-start(bf16[256,4096]{1,0:T(8,128)(2,1)} %param.12) | copy-start | bytes 6291460
  30.3 30.5 %copy-start.1 = (bf16[2,8,128,128]{3,2,1,0:T(8,128)(2,1)S(1)}, bf16[2,8,128,128]{3,2,1,0:T(8,128)(2,1)}, u32[]{:S(2)}) copy-start(bf16[2,8,128,128]{3,2,1,0:T(8,128)(2,1)} %mul.54) | copy-start | bytes 1572868
  30.3 30.5 %copy-start.2 = (bf16[2,8,128,128]{3,2,1,0:T(8,128)(2,1)S(1)}, bf16[2,8,128,128]{3,2,1,0:T(8,128)(2,1)}, u32[]{:S(2)}) copy-start(bf16[2,8,128,128]{3,2,1,0:T(8,128)(2,1)} %mul.61) | copy-start | bytes 1572868
Sparse Core Ops, SparseCore 0:
  9.1 48.3 all-gather.6
  59.1 44.4 all-gather.10
  105.1 44.4 all-gather.8
  151.0 45.1 all-gather.12

commit v2 on v0

v2 whole, which is shorter than its diff:
```python
import functools

import jax
import jax.numpy as jnp
from jax import lax
from jax.experimental import pallas as pl
from jax.experimental.pallas import tpu as pltpu
from jax.sharding import PartitionSpec as P

RG_C = 8.0
EPS = 0.1
MESH = pl.DeviceIdType.MESH
F32 = jnp.float32
BF16 = jnp.bfloat16
VM = pl.BlockSpec(memory_space=pltpu.VMEM)


def send(src, dst, send_sem, recv_sem, **device):
    return pltpu.make_async_remote_copy(
        src_ref=src,
        dst_ref=dst,
        send_sem=send_sem,
        recv_sem=recv_sem,
        device_id=device,
        device_id_type=MESH,
    )


def minus_expm1(x):
    series = 1.0 + x * (1.0 / 8.0)
    for n in range(7, 1, -1):
        series = 1.0 + (x * (1.0 / n)) * series
    return jnp.where(x > -0.5, -x * series, 1.0 - jnp.exp(x))


def whole_kernel(
    g, n_sp, n_tp,
    x_in, win_in, wout_in, doc_ref, gain_ref, taps_ref, bias_ref, rbias_ref, ibias_ref, coef_ref,
    rgate_ref, igate_ref,
    o_ref,
    xbuf, win, wout, part, gotten, tails, tail_out, doc_tail, docs, ext, a_buf, b_buf, ends, hid,
    psend, pgot,
    own_sem, x_send, x_recv, xt_send, xt_recv, w_send, w_recv, doc_sem, rs_send, rs_recv,
    tail_sem, end_send, end_recv, ag_send, ag_recv, tp_send, tp_recv, f_send, f_recv, ft_send,
    ft_recv,
):
    me = lax.axis_index("sp")
    core = lax.axis_index("tp")
    outer = n_sp // g
    inner, place = lax.rem(me, g), me // g
    base = place * g
    layers, width, chans = win_in.shape
    rows, features = xbuf.shape[1], xbuf.shape[2] * g
    taps = taps_ref.shape[1]
    half = rows // n_tp
    mine = pl.ds(core * half, half)
    strided = len(x_in.shape) == 2
    pieces = outer if strided else 1
    after = lax.rem(me + 1, n_sp)

    def piece(ref, at, j, o):
        if strided:
            return ref.at[at, pl.ds((o * g + j) * width, width)]
        return ref.at[j, at, :]

    def slot(ref, j, at, o):
        return ref.at[j, at, pl.ds(o * width, width)] if strided else ref.at[j, at, :]

    def weight(l, kind, o):
        if kind == 0:
            return win_in.at[l], win.at[l, pl.ds(o * width, width)]
        return wout_in.at[l], wout.at[l, o]

    line = outer == 4

    def weight_start(l, kind):
        k = 2 * l + kind
        src, dst = weight(l, kind, place)
        pltpu.make_async_copy(src, dst, own_sem.at[k]).start()
        for step in (2, 1, 3) if line else range(1, outer):
            to = lax.rem(place + step, outer)
            copy = send(src, dst, w_send.at[k, to], w_recv.at[k, place], sp=to * g + inner)
            if line:
                far = (place == 0) & (to == 3) | (place == 3) & (to == 0)
                pl.when(jnp.logical_not(far))(copy.start)
            else:
                copy.start()

    def weight_wait(l, kind, o):
        src, dst = weight(l, kind, o)
        k = 2 * l + kind
        send(src, dst, w_send.at[k, o], w_recv.at[k, o], sp=o * g + inner).wait_recv()

    def weight_relay(l, kind):
        if not line:
            return
        k = 2 * l + kind

        @pl.when((place == 1) | (place == 2))
        def _():
            o = jnp.where(place == 2, 0, 3)
            to = jnp.where(place == 2, 3, 0)
            weight_wait(l, kind, o)
            dst = weight(l, kind, o)[1]
            send(dst, dst, w_send.at[k, place], w_recv.at[k, o], sp=to * g + inner).start()

    def weight_done(l, kind):
        k = 2 * l + kind
        src, dst = weight(l, kind, place)
        pltpu.make_async_copy(src, dst, own_sem.at[k]).wait()
        for step in range(1, outer):
            o = lax.rem(place + step, outer)
            if line:
                taken = (place == 2) & (o == 0) | (place == 1) & (o == 3)
                pl.when(jnp.logical_not(taken))(functools.partial(weight_wait, l, kind, o))
            else:
                weight_wait(l, kind, o)

    def weight_close(l, kind):
        k = 2 * l + kind
        src, dst = weight(l, kind, place)
        for step in range(1, outer):
            to = lax.rem(place + step, outer)
            copy = send(src, dst, w_send.at[k, to], w_recv.at[k, place], sp=to * g + inner)
            if line:
                far = (place == 0) & (to == 3) | (place == 3) & (to == 0)
                pl.when(jnp.logical_not(far))(copy.wait_send)
            else:
                copy.wait_send()
        if line:
            copy = send(dst, dst, w_send.at[k, place], w_recv.at[k, place], sp=after)
            pl.when((place == 1) | (place == 2))(copy.wait_send)

    def x_copy(j, o, landed):
        return send(
            piece(x_in, mine, j, o),
            slot(xbuf, landed, mine, o),
            x_send.at[j, o],
            x_recv.at[landed, o],
            sp=base + j,
        )

    def x_go(step, _):
        j = lax.rem(inner + step, g)
        for o in range(pieces):
            x_copy(j, o, inner).start()
        return 0

    def own_piece(o):
        everything = pl.ds(0, rows)
        return pltpu.make_async_copy(
            piece(x_in, everything, inner, o),
            slot(xbuf, inner, everything, o),
            own_sem.at[2 * layers + o],
        )

    doc_copy = send(
        doc_ref.at[pl.ds(rows - 8, 8)], doc_tail, doc_sem.at[0], doc_sem.at[1], sp=after
    )
    weight_start(0, 0)
    lax.fori_loop(1, g, x_go, 0)
    doc_copy.start()
    for o in range(pieces):
        own_piece(o).start()

    def x_share(j, other, at):
        peer = lax.rem(core + other, n_tp)
        return send(
            xbuf.at[j, at], xbuf.at[j, at], xt_send.at[j, other - 1],
            xt_recv.at[j, n_tp - other - 1], tp=peer,
        )

    def x_arrive(step, _):
        j = lax.rem(inner + step, g)
        for o in range(pieces):
            x_copy(j, o, j).wait_recv()
        for other in range(1, n_tp):
            x_share(j, other, mine).start()
        return 0

    lax.fori_loop(1, g, x_arrive, 0)
    for o in range(pieces):
        own_piece(o).wait()
    weight_relay(0, 0)
    weight_start(0, 1)

    doc_copy.wait_recv()
    docs[pl.ds(0, 8), :] = jnp.where(me == 0, -1.0, doc_tail[...])
    docs[pl.ds(8, rows), :] = doc_ref[...]

    def x_shared(step, _):
        j = lax.rem(inner + step, g)
        for other in range(1, n_tp):
            peer = lax.rem(core + other, n_tp)
            at = pl.ds(peer * half, half)
            send(
                xbuf.at[j, at], xbuf.at[j, at], xt_send.at[j, other - 1],
                xt_recv.at[j, other - 1], tp=peer,
            ).wait_recv()
            x_share(j, other, mine).wait_send()
        for o in range(pieces):
            x_copy(j, o, inner).wait_send()
        return 0

    lax.fori_loop(1, g, x_shared, 0)
    doc_copy.wait_send()

    pair = 128
    dim = rgate_ref.shape[2]
    repeat = (
        lax.rem(lax.broadcasted_iota(jnp.int32, (dim, pair), 1), dim)
        == lax.broadcasted_iota(jnp.int32, (dim, pair), 0)
    ).astype(F32).astype(BF16)
    on_block = (
        lax.broadcasted_iota(jnp.int32, (pair, pair), 0) // dim
        == lax.broadcasted_iota(jnp.int32, (pair, pair), 1) // dim
    )

    def diagonal(ref, l, col):
        wide = jnp.dot(ref[l, pl.ds(col, pair), :], repeat, preferred_element_type=F32)
        return jnp.where(on_block, wide, 0.0).astype(BF16)

    for l in range(layers):
        last = l == layers - 1
        weight_done(l, 0)

        def project(step, _):
            j = lax.rem(inner + step, g)
            x = xbuf[j].astype(F32)
            squares = jnp.sum(x * x, axis=1, keepdims=True)
            high = squares.astype(BF16).astype(F32)
            lane = lax.broadcasted_iota(jnp.int32, (rows, 128), 1)
            extra = jnp.where(lane == 0, high, jnp.where(lane == 1, squares - high, 0.0))
            scaled = (x * gain_ref[l]).astype(BF16)
            out = jnp.dot(scaled, win[l], preferred_element_type=F32)
            part[j, :, :chans] = out.astype(BF16)
            part[j, :, chans:] = extra.astype(BF16)

            @pl.when(step < g)
            def _():
                send(
                    part.at[j], gotten.at[inner], rs_send.at[j], rs_recv.at[inner], sp=base + j
                ).start()

            return 0

        lax.fori_loop(1, g + 1, project, 0)
        ext[pl.ds(8, rows), :] = part[inner, :, :chans].astype(F32)
        sums = part[inner, :, chans:].astype(F32)

        def collect(step, sums):
            j = lax.rem(inner + step, g)
            send(part.at[j], gotten.at[j], rs_send.at[j], rs_recv.at[j], sp=base + j).wait_recv()
            ext[pl.ds(8, rows), :] += gotten[j, :, :chans].astype(F32)
            return sums + gotten[j, :, chans:].astype(F32)

        sums = lax.fori_loop(1, g, collect, sums)
        total = jnp.sum(sums, axis=1, keepdims=True)
        scale = lax.rsqrt(total * (1.0 / features) + EPS)
        mixed = (ext[pl.ds(8, rows), :] * scale).astype(BF16)
        tail_out[...] = mixed[rows - 16 :]
        tail_copy = send(
            tail_out, tails.at[l], tail_sem.at[l, 0], tail_sem.at[l, 1], sp=after
        )
        tail_copy.start()
        ext[pl.ds(8, rows), :] = mixed.astype(F32)
        weight_relay(l, 1)
        if not last:
            weight_start(l + 1, 0)
        tail_copy.wait_recv()
        ext[pl.ds(0, 8), :] = tails[l, 8:].astype(F32)

        for col in range(0, chans, pair):
            cols = pl.ds(col, pair)
            row = slice(l, l + 1)
            conv = bias_ref[row, cols] + taps_ref[l, 0:1, cols] * ext[pl.ds(8, rows), cols]
            for lag in range(1, taps):
                same = docs[pl.ds(8 - lag, rows), :] == docs[pl.ds(8, rows), :]
                shifted = ext[pl.ds(8 - lag, rows), cols]
                conv = conv + jnp.where(same, taps_ref[l, lag : lag + 1, cols] * shifted, 0.0)
            conv_out = conv.astype(BF16)
            recur = jnp.dot(conv_out, diagonal(rgate_ref, l, col), preferred_element_type=F32)
            inp = jnp.dot(conv_out, diagonal(igate_ref, l, col), preferred_element_type=F32)
            recur = jax.nn.sigmoid(recur + rbias_ref[row, cols])
            inp = jax.nn.sigmoid(inp + ibias_ref[row, cols])
            log_decay = coef_ref[row, cols] * recur
            keep = docs[pl.ds(7, rows), :] == docs[pl.ds(8, rows), :]
            a_buf[col // pair] = jnp.where(keep, jnp.exp(log_decay), 0.0)
            b_buf[col // pair] = jnp.sqrt(jnp.maximum(minus_expm1(2.0 * log_decay), 0.0)) * (
                inp * conv_out.astype(F32)
            )

        sub = rows // 8
        lanes = a_buf.shape[0]

        def advance(r, carry):
            at = pl.ds(r, 8, stride=sub)
            following = []
            for c in range(lanes):
                decay, state = carry[c]
                a = a_buf[c, at, :]
                decay = decay * a
                state = a * state + b_buf[c, at, :]
                a_buf[c, at, :] = decay
                b_buf[c, at, :] = state
                following.append((decay, state))
            return tuple(following)

        start = (jnp.ones((8, pair), F32), jnp.zeros((8, pair), F32))
        chunks = lax.fori_loop(0, sub, advance, (start,) * lanes, unroll=2)
        decay = jnp.concatenate([c[0] for c in chunks], axis=1)
        state = jnp.concatenate([c[1] for c in chunks], axis=1)
        prefix = [(jnp.ones((1, chans), F32), jnp.zeros((1, chans), F32))]
        for s in range(8):
            d, h = prefix[-1]
            prefix.append((d * decay[s : s + 1], decay[s : s + 1] * h + state[s : s + 1]))
        ends[l, me, 0:1, :] = prefix[8][0]
        ends[l, me, 1:2, :] = prefix[8][1]

        def end_copy(dst, src):
            return send(
                ends.at[l, me], ends.at[l, src], end_send.at[l, dst], end_recv.at[l, src], sp=dst
            )

        def end_to(dst, _):
            pl.when(dst > me)(lambda: end_copy(dst, me).start())
            return 0

        def end_close(dst, _):
            pl.when(dst > me)(lambda: end_copy(dst, me).wait_send())
            return 0

        def fold(src, state):
            pl.when(src < me)(lambda: end_copy(src, src).wait_recv())
            return jnp.where(src < me, ends[l, src, 0:1, :] * state + ends[l, src, 1:2, :], state)

        lax.fori_loop(0, n_sp, end_to, 0)
        carried = lax.fori_loop(0, n_sp, fold, jnp.zeros((1, chans), F32))
        for s in range(8):
            at = pl.ds(s * sub, sub)
            enter = prefix[s][0] * carried + prefix[s][1]
            for c in range(lanes):
                one = enter[:, c * pair : (c + 1) * pair]
                hid[inner, at, pl.ds(c * pair, pair)] = (
                    b_buf[c, at, :] + a_buf[c, at, :] * one
                ).astype(BF16)

        def ag_copy(j, landed):
            return send(
                hid.at[inner], hid.at[landed], ag_send.at[j], ag_recv.at[landed], sp=base + j
            )

        def spread(step, _):
            j = lax.rem(inner + step, g)
            ag_copy(j, inner).start()
            return 0

        lax.fori_loop(1, g, spread, 0)
        if not last:
            weight_relay(l + 1, 0)
            weight_start(l + 1, 1)
        weight_done(l, 1)

        def tp_copy(j, other, landed):
            peer = lax.rem(core + other, n_tp)
            return send(
                psend.at[j], pgot.at[l, landed, j], tp_send.at[other - 1, j],
                tp_recv.at[l, landed, j], tp=peer,
            )

        def unproject(step, _):
            j = lax.rem(inner + step, g)
            pl.when(step > 0)(lambda: ag_copy(j, j).wait_recv())
            h = hid[j]
            for block in range(outer):
                out = jnp.dot(h, wout[l, block], preferred_element_type=F32)
                psend[j, :, block * width : (block + 1) * width] = out.astype(BF16)
            for other in range(1, n_tp):
                tp_copy(j, other, n_tp - other - 1).start()
            return 0

        lax.fori_loop(0, g, unproject, 0)

        def f_copy(j, o, landed):
            return send(
                slot(xbuf, j, mine, o), piece(o_ref, mine, landed, o), f_send.at[j, o],
                f_recv.at[landed, o], sp=base + j,
            )

        def finish(step, _):
            j = lax.rem(inner + step, g)
            for other in range(1, n_tp):
                copy = tp_copy(j, other, other - 1)
                copy.wait_recv()
                copy.wait_send()
            at = mine if last else pl.ds(0, rows)
            summed = psend[j, at, :].astype(F32)
            for other in range(1, n_tp):
                summed = summed + pgot[l, other - 1, j, at, :].astype(F32)
            new = (xbuf[j, at, :].astype(F32) + summed).astype(BF16)
            xbuf[j, at, :] = new
            if last:

                @pl.when(step < g)
                def _():
                    for o in range(pieces):
                        f_copy(j, o, inner).start()

            return 0

        lax.fori_loop(1, g + 1, finish, 0)

        def close(step, _):
            j = lax.rem(inner + step, g)
            send(part.at[j], gotten.at[j], rs_send.at[j], rs_recv.at[j], sp=base + j).wait_send()
            ag_copy(j, j).wait_send()
            return 0

        lax.fori_loop(1, g, close, 0)
        tail_copy.wait_send()
        lax.fori_loop(0, n_sp, end_close, 0)

    for o in range(pieces):
        target = piece(o_ref, mine, inner, o)
        target[...] = slot(xbuf, inner, mine, o)[...]

    def f_arrive(step, _):
        j = lax.rem(inner + step, g)
        for o in range(pieces):
            f_copy(j, o, j).wait_recv()
        return 0

    lax.fori_loop(1, g, f_arrive, 0)

    def share_of(at):
        return o_ref.at[at] if strided else o_ref.at[:, at]

    def f_share(other, at, landed):
        return send(
            share_of(at), share_of(at), ft_send.at[other - 1], ft_recv.at[landed],
            tp=lax.rem(core + other, n_tp),
        )

    for other in range(1, n_tp):
        f_share(other, mine, n_tp - other - 1).start()
    for l in range(layers):
        weight_close(l, 0)
        weight_close(l, 1)

    def f_close(step, _):
        j = lax.rem(inner + step, g)
        for o in range(pieces):
            f_copy(j, o, inner).wait_send()
        return 0

    lax.fori_loop(1, g, f_close, 0)
    for other in range(1, n_tp):
        peer = lax.rem(core + other, n_tp)
        f_share(other, pl.ds(peer * half, half), other - 1).wait_recv()
        f_share(other, mine, other - 1).wait_send()


def per_device(
    g,
    tokens,
    documents,
    norm_gain,
    in_weight,
    conv_taps,
    conv_bias,
    recur_gate,
    input_gate,
    recur_bias,
    input_bias,
    decay_param,
    out_weight,
):
    n_sp, n_tp = lax.axis_size("sp"), lax.axis_size("tp")
    outer = n_sp // g
    rows, features = tokens.shape
    layers, width, chans = in_weight.shape
    inner = lax.rem(lax.axis_index("sp"), g)
    strided = width % 128 == 0
    pieces = outer if strided else 1
    part_width = outer * width

    docs = jnp.broadcast_to(documents.astype(F32)[:, None], (rows, 128))
    coef = -RG_C * jax.nn.softplus(-decay_param)
    gain = lax.dynamic_index_in_dim(norm_gain.reshape(layers, outer, g, width), inner, 2, False)
    gain = gain.reshape(layers, 1, part_width)
    dim = recur_gate.shape[2]
    x = tokens
    if not strided:
        x = x.reshape(rows, outer, g, width).transpose(2, 0, 1, 3).reshape(g, rows, part_width)
    dma = pltpu.SemaphoreType.DMA
    any_space = pl.BlockSpec(memory_space=pl.ANY)
    others = max(n_tp - 1, 1)
    out = pl.pallas_call(
        functools.partial(whole_kernel, g, n_sp, n_tp),
        out_shape=jax.ShapeDtypeStruct(x.shape, x.dtype),
        in_specs=[any_space] * 3 + [VM] * 9,
        out_specs=VM,
        scratch_shapes=[
            pltpu.VMEM((g, rows, part_width), BF16),
            pltpu.VMEM((layers, part_width, chans), BF16),
            pltpu.VMEM((layers, outer, chans, width), BF16),
            pltpu.VMEM((g, rows, chans + 128), BF16),
            pltpu.VMEM((g, rows, chans + 128), BF16),
            pltpu.VMEM((layers, 16, chans), BF16),
            pltpu.VMEM((16, chans), BF16),
            pltpu.VMEM((8, 128), F32),
            pltpu.VMEM((rows + 8, 128), F32),
            pltpu.VMEM((rows + 8, chans), F32),
            pltpu.VMEM((chans // 128, rows, 128), F32),
            pltpu.VMEM((chans // 128, rows, 128), F32),
            pltpu.VMEM((layers, n_sp, 2, chans), F32),
            pltpu.VMEM((g, rows, chans), BF16),
            pltpu.VMEM((g, rows, part_width), BF16),
            pltpu.VMEM((layers, others, g, rows, part_width), BF16),
            dma((2 * layers + pieces,)),
            dma((g, pieces)),
            dma((g, pieces)),
            dma((g, others)),
            dma((g, others)),
            dma((2 * layers, outer)),
            dma((2 * layers, outer)),
            dma((2,)),
            dma((g,)),
            dma((g,)),
            dma((layers, 2)),
            dma((layers, n_sp)),
            dma((layers, n_sp)),
            dma((g,)),
            dma((g,)),
            dma((others, g)),
            dma((layers, others, g)),
            dma((g, pieces)),
            dma((g, pieces)),
            dma((others,)),
            dma((others,)),
        ],
        compiler_params=pltpu.CompilerParams(
            has_side_effects=True, vmem_limit_bytes=60 * 1024 * 1024
        ),
    )(
        x, in_weight, out_weight, docs, gain, conv_taps, conv_bias, recur_bias, input_bias, coef,
        recur_gate.reshape(layers, chans, dim), input_gate.reshape(layers, chans, dim),
    )
    if not strided:
        out = out.reshape(g, rows, outer, width).transpose(1, 2, 0, 3).reshape(rows, features)
    return out


def solution(mesh):
    n_sp = mesh.shape["sp"]
    g = 4 if n_sp % 4 == 0 else 1
    return jax.shard_map(
        functools.partial(per_device, g),
        mesh=mesh,
        in_specs=(
            P("sp", None),
            P("sp"),
            P(),
            P(None, "sp", "tp"),
            P(None, None, "tp"),
            P(None, "tp"),
            P(None, "tp", None, None),
            P(None, "tp", None, None),
            P(None, "tp"),
            P(None, "tp"),
            P(None, "tp"),
            P(None, "tp", "sp"),
        ),
        out_specs=P("sp", None),
        check_vma=False,
    )
```

time: 762 us -> 254 us (0.33)
  Pallas kernels: 0 us -> 247 us
  waiting for transfers between devices: 229 us -> 0 us
  local copies, waits for them, and re-layouts: 206 us -> 5.29 us
  blocking collectives: 166 us -> 0 us
  other arithmetic: 89.8 us -> 1.99 us
  matrix products: 38.3 us -> 0 us
  between operations: 14.2 us -> 0.01 us
  starting transfers between devices: 11.6 us -> 0 us
    pallas_call x0 -> x1, Pallas kernels: none -> 247 us  [per_device(): pl.pallas_call(functools.partial(whole_kernel, g, n_sp, n_tp), out_shape=...]
    all_gather x2 -> x0, waiting for transfers between devices: 184 us -> none  [the longest x1 184 us: per_device(): lax.all_gather(in_weight, 'sp', axis=1, tiled=True)]
    all_gather x4 -> x0, blocking collectives: 166 us -> none  [carried_in(): gathered = jax.tree.map(lambda a: lax.all_gather(a, axis), part)]
    slice x112 -> x0, local copies, waits for them, and re-layouts: 148 us -> none  [the longest x104 145 us: per_device(): lax.associative_scan(combine, (decay_now, drive_term), axis=0)]
    add x53 -> x0, other arithmetic: 45 us -> none  [the longest x26 36.2 us: combine(): return (earlier[0] * following[0], following[0] * earlier[1] + following[1])]
    pad x56 -> x0, local copies, waits for them, and re-layouts: 42.5 us -> none  [per_device(): lax.associative_scan(combine, (decay_now, drive_term), axis=0)]
    psum x2 -> x0, waiting for transfers between devices: 40.8 us -> none  [per_device(): lax.psum(partial_sum.astype(jnp.bfloat16), 'tp').astype(jnp.float32)]
    dot_general x8 -> x0, matrix products: 38.3 us -> none  [the longest x2 16.9 us: per_device(): jnp.dot(hidden, whole_out[depth_at], preferred_element_type=jnp.float32)]
  transfers between devices with their start and end apart: 7 -> 0, of which waited for: 5 -> 0; matrix products, arithmetic and copies ran while one was open for 21% -> 0% of each run, Pallas kernels for 0% -> 0%
where the time goes in v2:
time: 254 us
  Pallas kernels  247 us (97%)
  local copies, waits for them, and re-layouts  5.29 us (2%)
    pallas_call x1, Pallas kernels, per_device(): pl.pallas_call(functools.partial(whole_kernel, g, n_sp, n_tp), out_shape=...  247 us

profile of v2, /device:TPU:0, one launch (start us, length us, event | category | flops | bytes accessed | tf_op | source)
XLA Modules:
  0.0 253.9 jit_solution(11260121568515096)
XLA Ops:
  0.0 0.7 convert_element_type.3
  0.7 1.3 fusion.coef_ref
  2.0 0.8 reshape.14
  2.8 0.6 constant_dynamic-slice_fusion
  3.4 0.8 broadcast_in_dim.2.doc_ref
  4.2 246.6 %shard_map.118 = bf16[256,4096]{1,0:T(8,128)(2,1)} custom-call(bf16[256,4096]{1,0:T(8,128)(2,1)} %x_in.1, bf16[2,256,1024]{2,1,0:T(8,128)(2,1)} %win_in.1, bf16[2,1024,256]{2,1,0:T(8,128)(2,1)} %wout_in.1, f32[256,128]{1,0:T(8,128)} %broadcast_in_dim.2.doc_ref, f32[2,1,1024]{2,1,0:T(1,128)} %bitcast.5, f32[2,4,1024]{2,1,0:T(4,128)} %taps_ref.1, ...), custom_call_target="tpu_custom_call" | custom-call | tf_op jit(solution)/shard_map/pallas_call | solution.py:498
  250.7 3.1 %copy.17 = bf16[256,4096]{1,0:T(8,128)(2,1)} copy(bf16[256,4096]{1,0:T(8,128)(2,1)} %shard_map.118) | data formatting | bytes 4194304

commit v3 on v2

--- a/solution.py
+++ b/solution.py
@@ -52,6 +52,7 @@
     layers, width, chans = win_in.shape
     rows, features = xbuf.shape[1], xbuf.shape[2] * g
     taps = taps_ref.shape[1]
+    halves, span = hid.shape[0], hid.shape[3]
     half = rows // n_tp
     mine = pl.ds(core * half, half)
     strided = len(x_in.shape) == 2
@@ -81,7 +82,7 @@
             to = lax.rem(place + step, outer)
             copy = send(src, dst, w_send.at[k, to], w_recv.at[k, place], sp=to * g + inner)
             if line:
-                far = (place == 0) & (to == 3) | (place == 3) & (to == 0)
+                far = (to - place) * (to - place) != 1
                 pl.when(jnp.logical_not(far))(copy.start)
             else:
                 copy.start()
@@ -98,6 +99,13 @@
 
         @pl.when((place == 1) | (place == 2))
         def _():
+            for way in (1, -1):
+                o, to = place - way, place + way
+                weight_wait(l, kind, o)
+                dst = weight(l, kind, o)[1]
+                send(
+                    dst, dst, w_send.at[k, outer + to], w_recv.at[k, o], sp=to * g + inner
+                ).start()
             o = jnp.where(place == 2, 0, 3)
             to = jnp.where(place == 2, 3, 0)
             weight_wait(l, kind, o)
@@ -111,7 +119,7 @@
         for step in range(1, outer):
             o = lax.rem(place + step, outer)
             if line:
-                taken = (place == 2) & (o == 0) | (place == 1) & (o == 3)
+                taken = (place == 1) | (place == 2)
                 pl.when(jnp.logical_not(taken))(functools.partial(weight_wait, l, kind, o))
             else:
                 weight_wait(l, kind, o)
@@ -123,13 +131,17 @@
             to = lax.rem(place + step, outer)
             copy = send(src, dst, w_send.at[k, to], w_recv.at[k, place], sp=to * g + inner)
             if line:
-                far = (place == 0) & (to == 3) | (place == 3) & (to == 0)
+                far = (to - place) * (to - place) != 1
                 pl.when(jnp.logical_not(far))(copy.wait_send)
             else:
                 copy.wait_send()
         if line:
             copy = send(dst, dst, w_send.at[k, place], w_recv.at[k, place], sp=after)
             pl.when((place == 1) | (place == 2))(copy.wait_send)
+            for way in (1, -1):
+                at = outer + lax.rem(place + way + outer, outer)
+                copy = send(dst, dst, w_send.at[k, at], w_recv.at[k, place], sp=after)
+                pl.when((place == 1) | (place == 2))(copy.wait_send)
 
     def x_copy(j, o, landed):
         return send(
@@ -224,141 +236,161 @@
         last = l == layers - 1
         weight_done(l, 0)
 
-        def project(step, _):
-            j = lax.rem(inner + step, g)
-            x = xbuf[j].astype(F32)
-            squares = jnp.sum(x * x, axis=1, keepdims=True)
-            high = squares.astype(BF16).astype(F32)
-            lane = lax.broadcasted_iota(jnp.int32, (rows, 128), 1)
-            extra = jnp.where(lane == 0, high, jnp.where(lane == 1, squares - high, 0.0))
-            scaled = (x * gain_ref[l]).astype(BF16)
-            out = jnp.dot(scaled, win[l], preferred_element_type=F32)
-            part[j, :, :chans] = out.astype(BF16)
-            part[j, :, chans:] = extra.astype(BF16)
-
-            @pl.when(step < g)
-            def _():
-                send(
-                    part.at[j], gotten.at[inner], rs_send.at[j], rs_recv.at[inner], sp=base + j
-                ).start()
-
-            return 0
-
-        lax.fori_loop(1, g + 1, project, 0)
-        ext[pl.ds(8, rows), :] = part[inner, :, :chans].astype(F32)
-        sums = part[inner, :, chans:].astype(F32)
-
-        def collect(step, sums):
-            j = lax.rem(inner + step, g)
-            send(part.at[j], gotten.at[j], rs_send.at[j], rs_recv.at[j], sp=base + j).wait_recv()
-            ext[pl.ds(8, rows), :] += gotten[j, :, :chans].astype(F32)
-            return sums + gotten[j, :, chans:].astype(F32)
-
-        sums = lax.fori_loop(1, g, collect, sums)
-        total = jnp.sum(sums, axis=1, keepdims=True)
-        scale = lax.rsqrt(total * (1.0 / features) + EPS)
-        mixed = (ext[pl.ds(8, rows), :] * scale).astype(BF16)
-        tail_out[...] = mixed[rows - 16 :]
-        tail_copy = send(
-            tail_out, tails.at[l], tail_sem.at[l, 0], tail_sem.at[l, 1], sp=after
-        )
-        tail_copy.start()
-        ext[pl.ds(8, rows), :] = mixed.astype(F32)
+        def rs_copy(h, j, landed):
+            lanes = pl.ds(0, span + 128 if h == 0 else span)
+            return send(
+                part.at[h, j, :, lanes], gotten.at[h, landed, :, lanes], rs_send.at[h, j],
+                rs_recv.at[h, landed], sp=base + j,
+            )
+
+        for h in range(halves):
+
+            def project(step, _):
+                j = lax.rem(inner + step, g)
+                if h == 0:
+                    x = xbuf[j].astype(F32)
+                    squares = jnp.sum(x * x, axis=1, keepdims=True)
+                    high = squares.astype(BF16).astype(F32)
+                    lane = lax.broadcasted_iota(jnp.int32, (rows, 128), 1)
+                    extra = jnp.where(lane == 0, high, jnp.where(lane == 1, squares - high, 0.0))
+                    psend[j] = (x * gain_ref[l]).astype(BF16)
+                    part[0, j, :, span:] = extra.astype(BF16)
+                out = jnp.dot(
+                    psend[j], win[l, :, h * span : (h + 1) * span], preferred_element_type=F32
+                )
+                part[h, j, :, :span] = out.astype(BF16)
+                pl.when(step < g)(lambda: rs_copy(h, j, inner).start())
+                return 0
+
+            lax.fori_loop(1, g + 1, project, 0)
         weight_relay(l, 1)
         if not last:
             weight_start(l + 1, 0)
-        tail_copy.wait_recv()
-        ext[pl.ds(0, 8), :] = tails[l, 8:].astype(F32)
-
-        for col in range(0, chans, pair):
-            cols = pl.ds(col, pair)
-            row = slice(l, l + 1)
-            conv = bias_ref[row, cols] + taps_ref[l, 0:1, cols] * ext[pl.ds(8, rows), cols]
-            for lag in range(1, taps):
-                same = docs[pl.ds(8 - lag, rows), :] == docs[pl.ds(8, rows), :]
-                shifted = ext[pl.ds(8 - lag, rows), cols]
-                conv = conv + jnp.where(same, taps_ref[l, lag : lag + 1, cols] * shifted, 0.0)
-            conv_out = conv.astype(BF16)
-            recur = jnp.dot(conv_out, diagonal(rgate_ref, l, col), preferred_element_type=F32)
-            inp = jnp.dot(conv_out, diagonal(igate_ref, l, col), preferred_element_type=F32)
-            recur = jax.nn.sigmoid(recur + rbias_ref[row, cols])
-            inp = jax.nn.sigmoid(inp + ibias_ref[row, cols])
-            log_decay = coef_ref[row, cols] * recur
-            keep = docs[pl.ds(7, rows), :] == docs[pl.ds(8, rows), :]
-            a_buf[col // pair] = jnp.where(keep, jnp.exp(log_decay), 0.0)
-            b_buf[col // pair] = jnp.sqrt(jnp.maximum(minus_expm1(2.0 * log_decay), 0.0)) * (
-                inp * conv_out.astype(F32)
+
+        sub = rows // 8
+        lanes = span // pair
+        scale = None
+        tail_copies, prefixes = [], []
+
+        def end_copy(h, dst, src):
+            return send(
+                ends.at[l, h, me], ends.at[l, h, src], end_send.at[l, h, dst],
+                end_recv.at[l, h, src], sp=dst,
             )
 
-        sub = rows // 8
-        lanes = a_buf.shape[0]
-
-        def advance(r, carry):
-            at = pl.ds(r, 8, stride=sub)
-            following = []
+        for h in range(halves):
+            ext[pl.ds(8, rows), :] = part[h, inner, :, :span].astype(F32)
+            sums = part[0, inner, :, span:].astype(F32)
+
+            def collect(step, sums):
+                j = lax.rem(inner + step, g)
+                rs_copy(h, j, j).wait_recv()
+                ext[pl.ds(8, rows), :] += gotten[h, j, :, :span].astype(F32)
+                return sums + gotten[0, j, :, span:].astype(F32)
+
+            sums = lax.fori_loop(1, g, collect, sums)
+            if h == 0:
+                total = jnp.sum(sums, axis=1, keepdims=True)
+                scale = lax.rsqrt(total * (1.0 / features) + EPS)
+            mixed = (ext[pl.ds(8, rows), :] * scale).astype(BF16)
+            tail_out[h] = mixed[rows - 16 :]
+            tail_copy = send(
+                tail_out.at[h], tails.at[l, h], tail_sem.at[l, h, 0], tail_sem.at[l, h, 1],
+                sp=after,
+            )
+            tail_copy.start()
+            tail_copies.append(tail_copy)
+            ext[pl.ds(8, rows), :] = mixed.astype(F32)
+            tail_copy.wait_recv()
+            ext[pl.ds(0, 8), :] = tails[l, h, 8:].astype(F32)
+
             for c in range(lanes):
-                decay, state = carry[c]
-                a = a_buf[c, at, :]
-                decay = decay * a
-                state = a * state + b_buf[c, at, :]
-                a_buf[c, at, :] = decay
-                b_buf[c, at, :] = state
-                following.append((decay, state))
-            return tuple(following)
-
-        start = (jnp.ones((8, pair), F32), jnp.zeros((8, pair), F32))
-        chunks = lax.fori_loop(0, sub, advance, (start,) * lanes, unroll=2)
-        decay = jnp.concatenate([c[0] for c in chunks], axis=1)
-        state = jnp.concatenate([c[1] for c in chunks], axis=1)
-        prefix = [(jnp.ones((1, chans), F32), jnp.zeros((1, chans), F32))]
-        for s in range(8):
-            d, h = prefix[-1]
-            prefix.append((d * decay[s : s + 1], decay[s : s + 1] * h + state[s : s + 1]))
-        ends[l, me, 0:1, :] = prefix[8][0]
-        ends[l, me, 1:2, :] = prefix[8][1]
-
-        def end_copy(dst, src):
-            return send(
-                ends.at[l, me], ends.at[l, src], end_send.at[l, dst], end_recv.at[l, src], sp=dst
-            )
-
-        def end_to(dst, _):
-            pl.when(dst > me)(lambda: end_copy(dst, me).start())
-            return 0
-
-        def end_close(dst, _):
-            pl.when(dst > me)(lambda: end_copy(dst, me).wait_send())
-            return 0
-
-        def fold(src, state):
-            pl.when(src < me)(lambda: end_copy(src, src).wait_recv())
-            return jnp.where(src < me, ends[l, src, 0:1, :] * state + ends[l, src, 1:2, :], state)
-
-        lax.fori_loop(0, n_sp, end_to, 0)
-        carried = lax.fori_loop(0, n_sp, fold, jnp.zeros((1, chans), F32))
-        for s in range(8):
-            at = pl.ds(s * sub, sub)
-            enter = prefix[s][0] * carried + prefix[s][1]
-            for c in range(lanes):
-                one = enter[:, c * pair : (c + 1) * pair]
-                hid[inner, at, pl.ds(c * pair, pair)] = (
-                    b_buf[c, at, :] + a_buf[c, at, :] * one
-                ).astype(BF16)
-
-        def ag_copy(j, landed):
-            return send(
-                hid.at[inner], hid.at[landed], ag_send.at[j], ag_recv.at[landed], sp=base + j
-            )
-
-        def spread(step, _):
-            j = lax.rem(inner + step, g)
-            ag_copy(j, inner).start()
-            return 0
-
-        lax.fori_loop(1, g, spread, 0)
+                here = pl.ds(c * pair, pair)
+                col = h * span + c * pair
+                cols = pl.ds(col, pair)
+                at = h * lanes + c
+                row = slice(l, l + 1)
+                conv = bias_ref[row, cols] + taps_ref[l, 0:1, cols] * ext[pl.ds(8, rows), here]
+                for lag in range(1, taps):
+                    same = docs[pl.ds(8 - lag, rows), :] == docs[pl.ds(8, rows), :]
+                    shifted = ext[pl.ds(8 - lag, rows), here]
+                    conv = conv + jnp.where(same, taps_ref[l, lag : lag + 1, cols] * shifted, 0.0)
+                conv_out = conv.astype(BF16)
+                recur = jnp.dot(conv_out, diagonal(rgate_ref, l, col), preferred_element_type=F32)
+                inp = jnp.dot(conv_out, diagonal(igate_ref, l, col), preferred_element_type=F32)
+                recur = jax.nn.sigmoid(recur + rbias_ref[row, cols])
+                inp = jax.nn.sigmoid(inp + ibias_ref[row, cols])
+                log_decay = coef_ref[row, cols] * recur
+                keep = docs[pl.ds(7, rows), :] == docs[pl.ds(8, rows), :]
+                a_buf[at] = jnp.where(keep, jnp.exp(log_decay), 0.0)
+                b_buf[at] = jnp.sqrt(jnp.maximum(minus_expm1(2.0 * log_decay), 0.0)) * (
+                    inp * conv_out.astype(F32)
+                )
+
+            def advance(r, carry):
+                at = pl.ds(r, 8, stride=sub)
+                following = []
+                for c in range(lanes):
+                    decay, state = carry[c]
+                    a = a_buf[h * lanes + c, at, :]
+                    decay = decay * a
+                    state = a * state + b_buf[h * lanes + c, at, :]
+                    a_buf[h * lanes + c, at, :] = decay
+                    b_buf[h * lanes + c, at, :] = state
+                    following.append((decay, state))
+                return tuple(following)
+
+            start = (jnp.ones((8, pair), F32), jnp.zeros((8, pair), F32))
+            chunks = lax.fori_loop(0, sub, advance, (start,) * lanes, unroll=4)
+            decay = jnp.concatenate([c[0] for c in chunks], axis=1)
+            state = jnp.concatenate([c[1] for c in chunks], axis=1)
+            prefix = [(jnp.ones((1, span), F32), jnp.zeros((1, span), F32))]
+            for s in range(8):
+                d, e = prefix[-1]
+                prefix.append((d * decay[s : s + 1], decay[s : s + 1] * e + state[s : s + 1]))
+            prefixes.append(prefix)
+            ends[l, h, me, 0:1, :] = prefix[8][0]
+            ends[l, h, me, 1:2, :] = prefix[8][1]
+
+            def end_to(dst, _):
+                pl.when(dst > me)(lambda: end_copy(h, dst, me).start())
+                return 0
+
+            lax.fori_loop(0, n_sp, end_to, 0)
+
         if not last:
             weight_relay(l + 1, 0)
             weight_start(l + 1, 1)
+
+        def ag_copy(h, j, landed):
+            return send(
+                hid.at[h, inner], hid.at[h, landed], ag_send.at[h, j], ag_recv.at[h, landed],
+                sp=base + j,
+            )
+
+        for h in range(halves):
+
+            def fold(src, state):
+                pl.when(src < me)(lambda: end_copy(h, src, src).wait_recv())
+                following = ends[l, h, src, 0:1, :] * state + ends[l, h, src, 1:2, :]
+                return jnp.where(src < me, following, state)
+
+            carried = lax.fori_loop(0, n_sp, fold, jnp.zeros((1, span), F32))
+            for s in range(8):
+                at = pl.ds(s * sub, sub)
+                enter = prefixes[h][s][0] * carried + prefixes[h][s][1]
+                for c in range(lanes):
+                    one = enter[:, c * pair : (c + 1) * pair]
+                    hid[h, inner, at, pl.ds(c * pair, pair)] = (
+                        b_buf[h * lanes + c, at, :] + a_buf[h * lanes + c, at, :] * one
+                    ).astype(BF16)
+
+            def spread(step, _):
+                j = lax.rem(inner + step, g)
+                ag_copy(h, j, inner).start()
+                return 0
+
+            lax.fori_loop(1, g, spread, 0)
         weight_done(l, 1)
 
         def tp_copy(j, other, landed):
@@ -370,10 +402,15 @@
 
         def unproject(step, _):
             j = lax.rem(inner + step, g)
-            pl.when(step > 0)(lambda: ag_copy(j, j).wait_recv())
-            h = hid[j]
+            for h in range(halves):
+                pl.when(step > 0)(lambda: ag_copy(h, j, j).wait_recv())
             for block in range(outer):
-                out = jnp.dot(h, wout[l, block], preferred_element_type=F32)
+                out = 0.0
+                for h in range(halves):
+                    out = out + jnp.dot(
+                        hid[h, j], wout[l, block, h * span : (h + 1) * span],
+                        preferred_element_type=F32,
+                    )
                 psend[j, :, block * width : (block + 1) * width] = out.astype(BF16)
             for other in range(1, n_tp):
                 tp_copy(j, other, n_tp - other - 1).start()
@@ -412,13 +449,21 @@
 
         def close(step, _):
             j = lax.rem(inner + step, g)
-            send(part.at[j], gotten.at[j], rs_send.at[j], rs_recv.at[j], sp=base + j).wait_send()
-            ag_copy(j, j).wait_send()
+            for h in range(halves):
+                rs_copy(h, j, j).wait_send()
+                ag_copy(h, j, j).wait_send()
             return 0
 
         lax.fori_loop(1, g, close, 0)
-        tail_copy.wait_send()
+
+        def end_close(dst, _):
+            for h in range(halves):
+                pl.when(dst > me)(lambda: end_copy(h, dst, me).wait_send())
+            return 0
+
         lax.fori_loop(0, n_sp, end_close, 0)
+        for tail_copy in tail_copies:
+            tail_copy.wait_send()
 
     for o in range(pieces):
         target = piece(o_ref, mine, inner, o)
@@ -483,6 +528,8 @@
     strided = width % 128 == 0
     pieces = outer if strided else 1
     part_width = outer * width
+    halves = 2 if chans % 256 == 0 else 1
+    span = chans // halves
 
     docs = jnp.broadcast_to(documents.astype(F32)[:, None], (rows, 128))
     coef = -RG_C * jax.nn.softplus(-decay_param)
@@ -504,17 +551,17 @@
             pltpu.VMEM((g, rows, part_width), BF16),
             pltpu.VMEM((layers, part_width, chans), BF16),
             pltpu.VMEM((layers, outer, chans, width), BF16),
-            pltpu.VMEM((g, rows, chans + 128), BF16),
-            pltpu.VMEM((g, rows, chans + 128), BF16),
-            pltpu.VMEM((layers, 16, chans), BF16),
-            pltpu.VMEM((16, chans), BF16),
+            pltpu.VMEM((halves, g, rows, span + 128), BF16),
+            pltpu.VMEM((halves, g, rows, span + 128), BF16),
+            pltpu.VMEM((layers, halves, 16, span), BF16),
+            pltpu.VMEM((halves, 16, span), BF16),
             pltpu.VMEM((8, 128), F32),
             pltpu.VMEM((rows + 8, 128), F32),
-            pltpu.VMEM((rows + 8, chans), F32),
+            pltpu.VMEM((rows + 8, span), F32),
             pltpu.VMEM((chans // 128, rows, 128), F32),
             pltpu.VMEM((chans // 128, rows, 128), F32),
-            pltpu.VMEM((layers, n_sp, 2, chans), F32),
-            pltpu.VMEM((g, rows, chans), BF16),
+            pltpu.VMEM((layers, halves, n_sp, 2, span), F32),
+            pltpu.VMEM((halves, g, rows, span), BF16),
             pltpu.VMEM((g, rows, part_width), BF16),
             pltpu.VMEM((layers, others, g, rows, part_width), BF16),
             dma((2 * layers + pieces,)),
@@ -522,16 +569,16 @@
             dma((g, pieces)),
             dma((g, others)),
             dma((g, others)),
-            dma((2 * layers, outer)),
-            dma((2 * layers, outer)),
+            dma((2 * layers, 2 * outer)),
+            dma((2 * layers, 2 * outer)),
             dma((2,)),
-            dma((g,)),
-            dma((g,)),
-            dma((layers, 2)),
-            dma((layers, n_sp)),
-            dma((layers, n_sp)),
-            dma((g,)),
-            dma((g,)),
+            dma((halves, g)),
+            dma((halves, g)),
+            dma((layers, halves, 2)),
+            dma((layers, halves, n_sp)),
+            dma((layers, halves, n_sp)),
+            dma((halves, g)),
+            dma((halves, g)),
             dma((others, g)),
             dma((layers, others, g)),
             dma((g, pieces)),

time: 254 us -> 224 us (0.88); the launches traced: 254 us -> 220 us
  Pallas kernels: 247 us -> 213 us
    pallas_call x1, Pallas kernels: 247 us -> 213 us  [per_device(): pl.pallas_call(functools.partial(whole_kernel, g, n_sp, n_tp), out_shape=...]
where the time goes in v3:
time: 224 us; the launch traced here: 220 us
  Pallas kernels  213 us (95%)
  local copies, waits for them, and re-layouts  5.29 us (2%)
    pallas_call x1, Pallas kernels, per_device(): pl.pallas_call(functools.partial(whole_kernel, g, n_sp, n_tp), out_shape=...  213 us

profile of v3, /device:TPU:0, one launch (start us, length us, event | category | flops | bytes accessed | tf_op | source)
XLA Modules:
  0.0 220.1 jit_solution(12224344535995757729)
XLA Ops:
  0.0 0.7 convert_element_type.3
  0.7 1.3 fusion.coef_ref
  2.0 0.8 reshape.14
  2.8 0.6 constant_dynamic-slice_fusion
  3.4 0.8 broadcast_in_dim.2.doc_ref
  4.2 212.8 %shard_map.118 = bf16[256,4096]{1,0:T(8,128)(2,1)} custom-call(bf16[256,4096]{1,0:T(8,128)(2,1)} %x_in.1, bf16[2,256,1024]{2,1,0:T(8,128)(2,1)} %win_in.1, bf16[2,1024,256]{2,1,0:T(8,128)(2,1)} %wout_in.1, f32[256,128]{1,0:T(8,128)} %broadcast_in_dim.2.doc_ref, f32[2,1,1024]{2,1,0:T(1,128)} %bitcast.5, f32[2,4,1024]{2,1,0:T(4,128)} %taps_ref.1, ...), custom_call_target="tpu_custom_call" | custom-call | tf_op jit(solution)/shard_map/pallas_call | solution.py:545
  217.0 3.1 %copy.17 = bf16[256,4096]{1,0:T(8,128)(2,1)} copy(bf16[256,4096]{1,0:T(8,128)(2,1)} %shard_map.118) | data formatting | bytes 4194304
